TPU v7x, 128 devices: a whole 4x4x4 slice. The times are simulated.
128 devices in a mesh: rep: 2 (over z_hi), fs: 32 (over z_lo, y, x), tp: 2 (over core).
Axes of the slice: x: 4, y: 4, z: 4 (z_hi: 2, z_lo: 2; z = z_hi * 2 + z_lo), core: 2. Of those that a mesh axis runs over, the one named last changes fastest.
Arguments:
- layer_in: bfloat16 [65536, 2048], P(('rep', 'fs'), 'tp'), may hold values from -60 to 60
- mix_gain: bfloat16 [2048], P('tp'), may hold values from 0.099609375 to 1.8984375
- pool_weight: float32 [4, 512, 512], P('tp', None, 'fs'), may hold values from -0.25 to 0.25
- pool_scale: float32 [4, 512], P('tp'), may hold values from 0.1 to 1.9
- out_weight: float32 [2048, 2048], P('tp', 'fs'), may hold values from -0.125 to 0.125
- out_scale: float32 [2048], P('tp'), may hold values from 0.1 to 1.9
- channel_gain: bfloat16 [2048], P('tp'), may hold values from 0.099609375 to 1.8984375
- up_weight: float32 [2048, 2816], P('fs', 'tp'), may hold values from -0.125 to 0.125
- up_scale: float32 [2816], P('tp'), may hold values from 0.1 to 1.9
- gate_weight: float32 [2048, 2816], P('fs', 'tp'), may hold values from -0.125 to 0.125
- gate_scale: float32 [2816], P('tp'), may hold values from 0.1 to 1.9
- conv_weight: float32 [3, 2816], P(None, 'tp'), may hold values from -3 to 3
- down_weight: float32 [2816, 2048], P('tp', 'fs'), may hold values from -0.109375 to 0.109375
- down_scale: float32 [2048], P('tp'), may hold values from 0.1 to 1.9
Outputs:
- layer_out: bfloat16 [65536, 2048], P(('rep', 'fs'), 'tp')
All inputs are finite; a program needn't handle non-finite values.
Results may differ from a plain program's by a relative error of at most 0.0095.
Values may be sent and summed in bfloat16 or wider, within the bound.
A program may use at most 128 MiB of HBM per device.

v0:
```python
import jax
import jax.numpy as jnp
from jax import lax
from jax.sharding import Mesh
from jax.sharding import PartitionSpec as P

LENGTH = 256
FS = ("fs_0", "fs_1", "fs_2")
REP_FS = ("rep", "fs_0", "fs_1", "fs_2")


EPS = 1e-06


def side_by_side(arrays, axis, dim, along):
    widths = [a.shape[along] for a in arrays]
    both = jnp.concatenate(arrays, axis=along)
    filled = lax.all_gather(both, axis, axis=dim, tiled=True)
    return tuple(jnp.split(filled, [sum(widths[:k]) for k in range(1, len(widths))], axis=along))


def in_order(parts, dim):
    dims = list(parts.shape[1:])
    dims[dim] *= parts.shape[0]
    return jnp.moveaxis(parts, 0, dim).reshape(dims)


def stacked_from(array, axes, turns):
    parts = array[None]
    for k in turns:
        parts = lax.all_gather(parts, axes[k], axis=0, tiled=True)
    held = [lax.axis_size(axes[k]) for k in reversed(turns)]
    parts = parts.reshape(*held, *array.shape)
    turned = sorted(range(len(turns)), key=lambda place: turns[len(turns) - 1 - place])
    return parts.transpose(*turned, *range(len(turns), parts.ndim)).reshape(-1, *array.shape)


def whole_of(array, axes, turns, dim):
    return in_order(stacked_from(array, axes, turns), dim)


def copy_for_each(array, axis):
    copies = jnp.broadcast_to(array, (lax.axis_size(axis), *array.shape))
    return lax.all_to_all(copies, axis, split_axis=0, concat_axis=0, tiled=True)


def over_copies(array, axis):
    return copy_for_each(array, axis).sum(axis=0)


def collect(array, axis, dim):
    return in_order(copy_for_each(array, axis), dim)


def cut_along(array, dim, peers):
    before, after = (array.shape[:dim], array.shape[dim + 1 :])
    return jnp.moveaxis(array.reshape(*before, peers, -1, *after), dim, 0)


def summed_on_arrival(array, axis, dim):
    parts = cut_along(array, dim, lax.axis_size(axis))
    arrived = lax.all_to_all(parts, axis, split_axis=0, concat_axis=0, tiled=True)
    return arrived.astype(jnp.float32).sum(axis=0)


def band_table(length, window):
    rows = lax.broadcasted_iota(jnp.int32, (length, length), 0)
    cols = lax.broadcasted_iota(jnp.int32, (length, length), 1)
    lower = jnp.maximum(rows - window // 2, 0)
    upper = jnp.minimum(rows - window // 2 + window, length)
    inside = (cols >= lower) & (cols < upper)
    count = (upper[:, :1] - lower[:, :1]).astype(jnp.float32)
    return (inside.astype(jnp.bfloat16), count)


def pool_groups(grouped_in, first_group):
    outputs = []
    for local in range(grouped_in.shape[2]):
        window = jnp.left_shift(jnp.int32(1), first_group + local + 1)
        band, count = band_table(grouped_in.shape[1], window)
        piece = grouped_in[:, :, local, :]
        total = jnp.einsum("ij,sjc->sic", band, piece, preferred_element_type=jnp.float32)
        outputs.append((total / count[None] - piece.astype(jnp.float32)).astype(jnp.bfloat16))
    return jnp.stack(outputs, axis=2)


def project_with(left, piece):
    return jnp.dot(left, piece, preferred_element_type=jnp.float32)


def per_device(
    layer_in,
    mix_gain,
    pool_weight,
    pool_scale,
    out_weight,
    out_scale,
    channel_gain,
    up_weight,
    up_scale,
    gate_weight,
    gate_scale,
    conv_weight,
    down_weight,
    down_scale,
):
    rows, half = layer_in.shape
    seqs = rows // LENGTH
    width = half * lax.axis_size("tp")
    up_bf = up_weight.astype(jnp.bfloat16)
    gate_bf = gate_weight.astype(jnp.bfloat16)
    down_bf = down_weight.astype(jnp.bfloat16)
    up_whole, gate_whole = side_by_side((up_bf, gate_bf), FS, 0, 1)
    down_whole = whole_of(down_bf, FS, (0, 1, 2), 1)
    x32 = layer_in.astype(jnp.float32)
    squares = over_copies(jnp.sum(x32 * x32, axis=1), "tp")
    normed = (
        x32 * lax.rsqrt(squares / width + EPS)[:, None] * mix_gain.astype(jnp.float32)[None]
    ).astype(jnp.bfloat16)
    local_groups = pool_weight.shape[0]
    group_width = half // local_groups
    first_group = lax.axis_index("tp") * local_groups
    pooled = pool_groups(normed.reshape(seqs, LENGTH, local_groups, group_width), first_group)
    grouped = jnp.einsum(
        "slgc,gcd->slgd",
        pooled,
        collect(pool_weight.astype(jnp.bfloat16), FS, 2),
        preferred_element_type=jnp.float32,
    )
    grouped = (grouped * pool_scale[None, None]).astype(jnp.bfloat16).reshape(rows, half)
    mixer_terms = project_with(
        grouped, lax.all_gather(out_weight.astype(jnp.bfloat16), FS, axis=1, tiled=True)
    )
    mixer_sum = summed_on_arrival(mixer_terms.astype(jnp.bfloat16), "tp", 1)
    middle = (x32 + mixer_sum * out_scale[None]).astype(jnp.bfloat16)
    m32 = middle.astype(jnp.float32)
    whole_middle, whole_gain = side_by_side((middle, channel_gain.reshape(1, half)), "tp", 1, 0)
    whole32 = whole_middle.astype(jnp.float32)
    chan_normed = (
        whole32
        * lax.rsqrt(jnp.mean(whole32 * whole32, axis=1, keepdims=True) + EPS)
        * whole_gain.astype(jnp.float32)
    ).astype(jnp.bfloat16)
    lifted_raw = jnp.dot(chan_normed, up_whole, preferred_element_type=jnp.float32)
    gated_raw = jnp.dot(chan_normed, gate_whole, preferred_element_type=jnp.float32)
    hidden_width = up_bf.shape[1]
    lifted = (lifted_raw * up_scale[None]).astype(jnp.bfloat16)
    padded = jnp.pad(
        lifted.reshape(seqs, LENGTH, hidden_width).astype(jnp.float32), ((0, 0), (1, 1), (0, 0))
    )
    conv = (
        conv_weight[0] * padded[:, :-2]
        + conv_weight[1] * padded[:, 1:-1]
        + conv_weight[2] * padded[:, 2:]
    )
    hidden = (
        jax.nn.gelu(conv).reshape(rows, hidden_width) * (gated_raw * gate_scale[None])
    ).astype(jnp.bfloat16)
    chan_terms = jnp.dot(hidden, down_whole, preferred_element_type=jnp.float32)
    chan_sum = summed_on_arrival(chan_terms.astype(jnp.bfloat16), "tp", 1)
    return (m32 + chan_sum * down_scale[None]).astype(jnp.bfloat16)


def solution(mesh):
    torus = Mesh(
        mesh.devices.reshape(mesh.shape["rep"], 2, 4, 4, mesh.shape["tp"]),
        ("rep", "fs_0", "fs_1", "fs_2", "tp"),
    )
    in_specs = (
        P(REP_FS, "tp"),
        P("tp"),
        P("tp", None, FS),
        P("tp", None),
        P("tp", FS),
        P("tp"),
        P("tp"),
        P(FS, "tp"),
        P("tp"),
        P(FS, "tp"),
        P("tp"),
        P(None, "tp"),
        P("tp", FS),
        P("tp"),
    )
    out_specs = P(REP_FS, "tp")
    return jax.shard_map(
        per_device, mesh=torus, in_specs=in_specs, out_specs=out_specs, check_vma=False
    )
```

profile of v0, /device:TPU:1, one launch (start us, length us, event | category | flops | bytes accessed | tf_op | source)
XLA Modules:
  0.0 511.4 jit_solution(16965219766778165992)
XLA Ops:
  6.5 1.2 convert_element_type.126
  7.7 7.4 %all-gather = bf16[2816,64]{0,1:T(8,128)(2,1)S(1)} all-gather(bf16[1408,64]{0,1:T(8,128)(2,1)S(1)} %convert_element_type.126), channel_id=2, replica_groups=mesh['rep'=2,'fs_0'=2,'fs_1'=4,'fs_2'=4,'tp'=2] {'fs_0'}, dimensions={0}, use_global_device_ids=true | all-gather | bytes 540672 | tf_op jit(solution)/shard_map/all_gather | solution.py:31
  15.1 0.8 copy.92
  15.8 0.0 all-gather.13.cloned.1.call-update
  15.9 0.0 all-gather.7.cloned.1.call-start
  15.9 1.6 convert_element_type.113
  17.5 0.0 all-gather.7.cloned.1.call-update
  17.5 0.0 all-gather.15.cloned.1.call-start
  17.6 26.4 %all-gather.13.cloned.1.call-done = bf16[8,1408,64]{1,2,0:T(8,128)(2,1)} async-done(((bf16[2,1408,64]{1,2,0:T(8,128)(2,1)}), bf16[8,1408,64]{1,2,0:T(8,128)(2,1)}) %all-gather.13.cloned.1.call-update) | async-done | bytes 1441808 | tf_op jit(solution)/shard_map/all_gather | solution.py:31
  44.0 0.0 all-gather.15.cloned.1.call-update
  44.1 0.5 fusion.19
  44.5 0.6 broadcast_in_dim.6
  45.1 4.1 all-to-all-start
  49.2 1.0 all-to-all-done
  50.2 1.1 broadcast_in_dim.7
  51.3 6.9 %all-to-all-start.1 = ((bf16[32,2,512,16]{2,3,1,0:T(8,128)(2,1)}), bf16[32,2,512,16]{2,3,1,0:T(8,128)(2,1)S(1)}, u32[]{:S(2)}, u32[]{:S(2)}) async-start(bf16[32,2,512,16]{2,3,1,0:T(8,128)(2,1)} %broadcast_in_dim.7), calls=%async_computation.1 | async-start | bytes 2097152 | tf_op jit(solution)/shard_map/all_to_all | solution.py:44
  58.3 0.0 all-gather.9.cloned.1.call-start
  58.3 1.9 fusion.21
  60.2 3.3 reshape.83
  63.5 4.2 fusion.50
  67.7 5.9 %copy.81 = bf16[4,256,1,512]{1,3,0,2:T(8,128)(2,1)} copy(bf16[4,256,1,512]{3,2,1,0:T(2,128)(2,1)} %get-tuple-element.8) | data formatting | bytes 2097152
  73.6 3.7 copy.82
  77.4 0.0 copy-start.4
  77.4 2.2 fusion.31
  79.6 0.0 copy-start.15
  79.7 1.5 fusion.32
  81.2 0.0 all-to-all-done.1
  81.2 0.1 copy.68
  81.3 2.9 fusion.28
  84.1 2.2 copy.71
  86.3 0.6 copy.86
  86.9 102.2 %all-gather.7.cloned.1.call-done = bf16[1024,2048]{0,1:T(8,128)(2,1)} async-done(((bf16[1024,64]{0,1:T(8,128)(2,1)}), bf16[1024,2048]{0,1:T(8,128)(2,1)}) %all-gather.7.cloned.1.call-update) | async-done | bytes 4194320 | tf_op jit(solution)/shard_map/all_gather | solution.py:132
  189.1 6.9 %convolution_convert_fusion.1 = bf16[1024,2048]{1,0:T(8,128)(2,1)S(1)} fusion(bf16[1024,1024]{1,0:T(8,128)(2,1)S(1)} %bitcast.88, bf16[1024,2048]{0,1:T(8,128)(2,1)} %all-gather.7.cloned.1.call-done), kind=kOutput, calls=%fused_computation.34 | convolution fusion | flops 4297064448 | bytes 10485760 | tf_op jit(solution)/shard_map/dot_general | solution.py:88
  196.1 0.5 copy.91
  196.6 25.8 %all_to_all.21 = bf16[2,1024,1024]{2,1,0:T(8,128)(2,1)S(1)} all-to-all(bf16[2,1024,1024]{2,1,0:T(8,128)(2,1)S(1)} %bitcast.78), channel_id=1, replica_groups=mesh['rep'=2,'fs_0'=2,'fs_1'=4,'fs_2'=4,'tp'=2] {'tp'}, dimensions={0} | all-to-all | bytes 8388608 | tf_op jit(solution)/shard_map/all_to_all | solution.py:62
  222.4 1.1 convert_reduce_fusion.1
  223.5 0.6 copy-done.1
  224.0 0.8 fusion.22
  224.9 0.0 copy-start.5
  224.9 0.0 copy-start.6
  224.9 0.0 copy-start.8
  224.9 1.5 pad_maximum_fusion
  226.4 0.0 all-gather.9.cloned.1.call-update
  226.5 0.2 all-gather.11.cloned.1.call-start
  226.8 0.8 pad_maximum_fusion.1
  227.5 0.0 all-gather.11.cloned.1.call-update
  227.6 0.1 slice_reduce_fusion.2
  227.6 42.2 %all-gather.15.cloned.1.call-done = bf16[32,1408,64]{1,2,0:T(8,128)(2,1)} async-done(((bf16[8,1408,64]{1,2,0:T(8,128)(2,1)}), bf16[32,1408,64]{1,2,0:T(8,128)(2,1)}) %all-gather.15.cloned.1.call-update) | async-done | bytes 5767184 | tf_op jit(solution)/shard_map/all_gather | solution.py:31
  269.9 5.7 %copy.74 = bf16[2,4,4,1408,64]{3,4,2,1,0:T(8,128)(2,1)} copy(bf16[2,4,4,1408,64]{3,4,0,1,2:T(8,128)(2,1)} %bitcast.81) | data formatting | bytes 11534336 | tf_op jit(solution)/shard_map/transpose | solution.py:35
  275.6 13.4 %all-gather.9.cloned.1.call-done = bf16[1025,2048]{1,0:T(8,128)(2,1)} async-done(((bf16[1025,1024]{1,0:T(8,128)(2,1)}), bf16[1025,2048]{1,0:T(8,128)(2,1)}) %all-gather.9.cloned.1.call-update) | async-done | bytes 4198416 | tf_op jit(solution)/shard_map/all_gather | solution.py:18
  289.0 3.1 fusion
  292.1 0.8 slice_convert_fusion
  292.8 151.2 %all-gather.11.cloned.1.call-done = bf16[2048,2816]{1,0:T(8,128)(2,1)} async-done(((bf16[64,2816]{1,0:T(8,128)(2,1)}), bf16[2048,2816]{1,0:T(8,128)(2,1)}) %all-gather.11.cloned.1.call-update) | async-done | bytes 11534352 | tf_op jit(solution)/shard_map/all_gather | solution.py:18
  444.1 10.4 %multiply_convert_fusion = bf16[1024,1408]{1,0:T(8,128)(2,1)S(1)} fusion(bf16[2048,2816]{1,0:T(8,128)(2,1)} %all-gather.11.cloned.1.call-done, f32[1408]{0:T(1024)S(1)} %copy-done.13, f32[2048]{0:T(1024)S(1)} %bitcast.92, f32[1024]{0:T(1024)S(1)} %add_rsqrt_fusion, bf16[1025,2048]{1,0:T(8,128)(2,1)} %all-gather.9.cloned.1.call-done), kind=kOutput, calls=%fused_computation.24 | convolution fusion | flops 5916852224 | bytes 12862976 | tf_op jit(solution)/shard_map/dot_general | solution.py:144
  454.5 0.4 convert.2
  454.9 0.0 copy-start.14
  454.9 3.4 fusion.9
  458.3 0.0 slice-start.1
  458.3 9.0 %fusion.14 = bf16[1024,1408]{1,0:T(8,128)(2,1)S(1)} fusion(f32[4,256,1408]{2,1,0:T(8,128)S(1)} %fusion.9, bf16[2048,2816]{1,0:T(8,128)(2,1)} %all-gather.11.cloned.1.call-done, f32[1408]{0:T(1024)S(1)} %copy-done.14, f32[2048]{0:T(1024)S(1)} %bitcast.93, f32[1024]{0:T(1024)S(1)} %add_rsqrt_fusion, bf16[1025,2048]{1,0:T(8,128)(2,1)S(1)} %copy-done.3), kind=kOutput, calls=%fused_computation.23 | convolution fusion | flops 5918294016 | bytes 18632704 | tf_op jit(solution)/shard_map/dot_general | solution.py:145
  467.4 6.9 %convolution_convert_fusion = bf16[1024,2048]{1,0:T(8,128)(2,1)S(1)} fusion(bf16[1024,1408]{1,0:T(8,128)(2,1)S(1)} %fusion.14, bf16[1408,2048]{0,1:T(8,128)(2,1)S(1)} %bitcast.84), kind=kOutput, calls=%fused_computation.33 | convolution fusion | flops 5907677184 | bytes 12845056 | tf_op jit(solution)/shard_map/dot_general | solution.py:159
  474.3 0.4 copy.90
  474.8 26.8 %all_to_all.22 = bf16[2,1024,1024]{2,1,0:T(8,128)(2,1)S(1)} all-to-all(bf16[2,1024,1024]{2,1,0:T(8,128)(2,1)S(1)} %bitcast.79), channel_id=1, replica_groups=mesh['rep'=2,'fs_0'=2,'fs_1'=4,'fs_2'=4,'tp'=2] {'tp'}, dimensions={0} | all-to-all | bytes 8388608 | tf_op jit(solution)/shard_map/all_to_all | solution.py:62
  501.6 1.0 convert_reduce_fusion
  502.7 2.2 add_convert_fusion
  (42 shorter events, 0.2 us)
Async XLA Ops:
  6.5 37.5 %copy-start = (bf16[1024,1024]{1,0:T(8,128)(2,1)S(1)}, bf16[1024,1024]{1,0:T(8,128)(2,1)}, u32[]{:S(2)}) copy-start(bf16[1024,1024]{1,0:T(8,128)(2,1)} %param.14) | copy-start | bytes 6291460
  6.5 42.7 %copy-start.11 = (bf16[1024]{0:T(1024)(128)(2,1)S(1)}, bf16[1024]{0:T(1024)(128)(2,1)}, u32[]{:S(2)}) copy-start(bf16[1024]{0:T(1024)(128)(2,1)} %param.15) | copy-start | bytes 6148
  6.5 42.7 %copy-start.7 = (f32[2,512,16]{1,2,0:T(8,128)S(1)}, f32[2,512,16]{1,2,0:T(8,128)}, u32[]{:S(2)}) copy-start(f32[2,512,16]{1,2,0:T(8,128)} %param.16) | copy-start | bytes 196612
  6.5 37.5 %all-gather.13.cloned.1.call-start = ((), (), s32[]{:S(2)}) async-start(), calls=%async_computation.7 | async-start | bytes 1802240 | tf_op jit(solution)/shard_map/all_gather | solution.py:31
  15.9 173.3 %all-gather.7.cloned.1.call-start = ((), (), s32[]{:S(2)}) async-start(), calls=%async_computation.4 | async-start | bytes 4325376 | tf_op jit(solution)/shard_map/all_gather | solution.py:132
  17.5 252.3 %all-gather.15.cloned.1.call-start = ((), (), s32[]{:S(2)}) async-start(), calls=%async_computation.8 | async-start | bytes 7208960 | tf_op jit(solution)/shard_map/all_gather | solution.py:31
  45.1 5.1 all-to-all-start
  51.3 29.8 %all-to-all-start.1 = ((bf16[32,2,512,16]{2,3,1,0:T(8,128)(2,1)}), bf16[32,2,512,16]{2,3,1,0:T(8,128)(2,1)S(1)}, u32[]{:S(2)}, u32[]{:S(2)}) async-start(bf16[32,2,512,16]{2,3,1,0:T(8,128)(2,1)} %broadcast_in_dim.7), calls=%async_computation.1 | async-start | bytes 2097152 | tf_op jit(solution)/shard_map/all_to_all | solution.py:44
  58.3 230.7 %all-gather.9.cloned.1.call-start = ((), (), s32[]{:S(2)}) async-start(), calls=%async_computation.5 | async-start | bytes 6340608 | tf_op jit(solution)/shard_map/all_gather | solution.py:18
  67.7 5.9 %copy-start.2 = (bf16[4,256,1,512]{3,2,1,0:T(2,128)(2,1)S(1)}, bf16[4,256,1,512]{3,2,1,0:T(2,128)(2,1)}, u32[]{:S(2)}) copy-start(bf16[4,256,1,512]{3,2,1,0:T(2,128)(2,1)} %get-tuple-element.9) | copy-start | bytes 3145732
  67.7 9.7 %copy-start.12 = (bf16[1024]{0:T(1024)(128)(2,1)S(1)}, bf16[1024]{0:T(1024)(128)(2,1)}, u32[]{:S(2)}) copy-start(bf16[1024]{0:T(1024)(128)(2,1)} %param.20) | copy-start | bytes 6148
  77.4 2.2 copy-start.4
  79.6 1.6 copy-start.15
  222.4 1.6 copy-start.1
  222.4 1.6 copy-start.9
  224.9 1.8 copy-start.5
  224.9 1.8 copy-start.6
  224.9 2.7 copy-start.8
  226.5 217.6 %all-gather.11.cloned.1.call-start = ((), (), s32[]{:S(2)}) async-start(), calls=%async_computation.6 | async-start | bytes 11894784 | tf_op jit(solution)/shard_map/all_gather | solution.py:18
  275.6 168.5 %copy-start.13 = (f32[1408]{0:T(1024)S(1)}, f32[1408]{0:T(1024)}, u32[]{:S(2)}) copy-start(f32[1408]{0:T(1024)} %param.22) | copy-start | bytes 16900
  454.9 3.5 copy-start.3
  454.9 3.5 copy-start.14
  454.9 12.5 %slice-start = ((s8[5767168]{0:T(1024)(128)(4,1)}), s8[4194304]{0:T(1024)(128)(4,1)S(1)}, s32[]{:S(2)}) async-start(s8[5767168]{0:T(1024)(128)(4,1)} %bitcast.82), calls=%async_computation.9 | async-start | bytes 8388608
  458.3 9.0 %slice-start.1 = ((s8[5767168]{0:T(1024)(128)(4,1)}), s8[1572864]{0:T(1024)(128)(4,1)S(1)}, s32[]{:S(2)}) async-start(s8[5767168]{0:T(1024)(128)(4,1)} %bitcast.82), calls=%async_computation.10 | async-start | bytes 3145728
  501.6 1.0 copy-start.10
Sparse Core Ops, SparseCore 0:
  16.0 27.9 all-gather.12
  45.7 143.4 all-gather.6
  190.8 79.0 all-gather.14
  271.4 17.5 all-gather.8
  290.5 153.5 all-gather.10
where the time goes:
time: 512 us; the launch traced here: 511 us
  waiting for transfers between devices  337 us (66%)
  blocking collectives  60 us (12%)
  matrix products  39.8 us (8%)
  local copies, waits for them, and re-layouts  29.8 us (6%)
  other arithmetic  20.3 us (4%)
  between operations  13.6 us (3%)
  starting transfers between devices  11.3 us (2%)
    all_gather x2, waiting for transfers between devices, side_by_side(): filled = lax.all_gather(both, axis, axis=dim, tiled=True)  165 us
    all_gather x1, waiting for transfers between devices, per_device(): lax.all_gather(out_weight.astype(jnp.bfloat16), FS, axis=1, tiled=True)  102 us
    all_gather x2, waiting for transfers between devices, stacked_from(): parts = lax.all_gather(parts, axes[k], axis=0, tiled=True)  68.7 us
    all_to_all x2, blocking collectives, summed_on_arrival(): lax.all_to_all(parts, axis, split_axis=0, concat_axis=0, tiled=True)  52.6 us
    all_to_all x2, starting transfers between devices, copy_for_each(): return lax.all_to_all(copies, axis, split_axis=0, concat_axis=0, tiled=True)  11 us
    unnamed x39, local copies, waits for them, and re-layouts  10.9 us
    dot_general x1, matrix products, per_device(): jnp.dot(chan_normed, up_whole, preferred_element_type=jnp.float32)  10.4 us
  transfers between devices with their start and end apart: 7, of which 6 were waited for; matrix products, arithmetic and copies ran while one was open for 10% of the time, Pallas kernels for 0%

commit v1 on v0

v1 whole, which is shorter than its diff:
```python
import functools

import jax
import jax.numpy as jnp
from jax import lax
from jax.experimental import pallas as pl
from jax.experimental.pallas import tpu as pltpu
from jax.sharding import Mesh
from jax.sharding import PartitionSpec as P

LENGTH = 256
FS = ("fs_0", "fs_1", "fs_2")
REP_FS = ("rep", "fs_0", "fs_1", "fs_2")
EPS = 1e-06

F32 = jnp.float32
BF16 = jnp.bfloat16
MESH = pl.DeviceIdType.MESH

ROWS = 1024
HALF = 1024
WIDTH = 2048
HID = 1408
SEQS = ROWS // LENGTH
LANES = 128

U_POOL = 0
U_OUT = 2
U_LAST = 10
U_FF = 12
U_DOWN = 32
UNITS = 43
COLOURS = 4
CHUNKS = 11
STAGES = 5
SLOTS = CHUNKS + STAGES

ORDERS = (("x", "y", "z"), ("y", "x", "z"), ("x", "z", "y"), ("y", "z", "x"))
STEPS = (
    ((0, "a"), (0, "b"), (1, "a"), (1, "b"), (2, "a")),
    ((0, "a"), (0, "b"), (1, "a"), (1, "b"), (2, "a")),
    ((0, "a"), (0, "b"), (1, "a"), (2, "a"), (2, "b")),
    ((0, "a"), (0, "b"), (1, "a"), (2, "a"), (2, "b")),
)
AXIS = {"x": "fs_2", "y": "fs_1"}


def dot_nt(left, right):
    return lax.dot_general(left, right, (((1,), (1,)), ((), ())), preferred_element_type=F32)


def kernel(
    x_hbm,
    pool_hbm,
    out_hbm,
    up_hbm,
    gate_hbm,
    down_hbm,
    prm_hbm,
    ffp_hbm,
    y_hbm,
    w,
    x,
    mixed,
    give,
    got,
    own,
    mid,
    normed,
    hid,
    acc,
    st_pool,
    st_out,
    st_up,
    st_gate,
    st_down,
    prm,
    ffp,
    sq,
    in_sem,
    send_sem,
    recv_sem,
    tp_send,
    tp_recv,
    y_sem,
):
    rep = lax.axis_index("rep")
    zl = lax.axis_index("fs_0")
    me = {"z": zl, "y": lax.axis_index("fs_1"), "x": lax.axis_index("fs_2")}
    tp = lax.axis_index("tp")
    mate = 1 - tp
    zz = rep * 2 + zl
    z_up = lax.rem(zz + 1, 4)
    z_down = lax.rem(zz + 3, 4)

    def to_z(place):
        return {"rep": place // 2, "fs_0": lax.rem(place, 2)}

    def ring(dim, shift):
        return lax.rem(me[dim] + shift + 4, 4)

    peers = [to_z(z_up), to_z(z_down), {"tp": mate}]
    for dim in ("x", "y"):
        peers += [{AXIS[dim]: ring(dim, 1)}, {AXIS[dim]: ring(dim, -1)}]

    loads = [
        pltpu.make_async_copy(src, dst, in_sem.at[k])
        for k, (src, dst) in enumerate(
            (
                (pool_hbm, st_pool),
                (out_hbm, st_out),
                (up_hbm, st_up),
                (gate_hbm, st_gate),
                (down_hbm, st_down),
                (x_hbm, x),
                (prm_hbm, prm.at[tp]),
                (ffp_hbm, ffp),
            )
        )
    ]
    for load in loads:
        load.start()

    barrier = pltpu.get_barrier_semaphore()
    for peer in peers:
        pl.semaphore_signal(barrier, inc=1, device_id=peer, device_id_type=MESH)

    for load in loads:
        load.wait()

    mine = (me["z"], me["y"], me["x"])
    for g in range(2):
        for ct in range(4):
            block = st_pool[g, ct * LANES : (ct + 1) * LANES, :]
            w[(U_POOL + g, *mine, pl.ds(ct * 16, 16), slice(None))] = block.T.astype(BF16)
    for k in range(8):
        w[(U_OUT + k, *mine)] = st_out[k * LANES : (k + 1) * LANES, :].T.astype(BF16)
    for k in range(11):
        w[(U_DOWN + k, *mine)] = st_down[k * LANES : (k + 1) * LANES, :].T.astype(BF16)
        columns = slice(k * LANES, (k + 1) * LANES)
        at_up = U_LAST if k == 10 else U_FF + 4 * (k // 2) + k % 2
        at_gate = U_LAST + 1 if k == 10 else U_FF + 4 * (k // 2) + 2 + k % 2
        w[(at_up, *mine)] = st_up[:, columns].astype(BF16)
        w[(at_gate, *mine)] = st_gate[:, columns].astype(BF16)

    pl.semaphore_wait(barrier, len(peers))

    def across(src, dst, index):
        return pltpu.make_async_remote_copy(
            src_ref=src,
            dst_ref=dst,
            send_sem=tp_send.at[index],
            recv_sem=tp_recv.at[index],
            device_id={"tp": mate},
            device_id_type=MESH,
        )

    across(prm_hbm, prm.at[tp], 0).start()

    def region(u, order, phase, place, rows):
        picks = {}
        for k, dim in enumerate(order):
            if k < phase:
                picks[dim] = slice(None)
            elif k == phase:
                picks[dim] = pl.ds(place, 1)
            else:
                picks[dim] = pl.ds(me[dim], 1)
        return w.at[u, picks["z"], picks["y"], picks["x"], rows, :]

    every, first, second = pl.ds(0, 64), pl.ds(0, 32), pl.ds(32, 32)

    def moves(colour, stage):
        order = ORDERS[colour]
        phase, step = STEPS[colour][stage]
        dim = order[phase]
        if dim == "z":
            there = 1 - zl
            return phase, (
                (zl, first, to_z(z_up), there, first),
                (zl, second, to_z(z_down), there, second),
            )
        right, left = {AXIS[dim]: ring(dim, 1)}, {AXIS[dim]: ring(dim, -1)}
        if step == "a":
            return phase, (
                (me[dim], every, right, ring(dim, -1), every),
                (me[dim], every, left, ring(dim, 1), every),
            )
        return phase, (
            (ring(dim, -1), first, right, ring(dim, 2), first),
            (ring(dim, 1), second, left, ring(dim, 2), second),
        )

    def hop(colour, stage, chunk, direction, arriving):
        u = chunk * COLOURS + colour
        phase, both = moves(colour, stage)
        place, rows, peer, from_place, from_rows = both[direction]
        if arriving:
            place, rows = from_place, from_rows
        ref = region(u, ORDERS[colour], phase, place, rows)
        return pltpu.make_async_remote_copy(
            src_ref=ref,
            dst_ref=ref,
            send_sem=send_sem.at[u],
            recv_sem=recv_sem.at[u, stage, direction],
            device_id=peer,
            device_id_type=MESH,
        )

    def advance(colour, slot):
        for depth in (0, 5, 4, 3, 2, 1):
            chunk = slot - depth

            @pl.when((chunk >= 0) & (chunk * COLOURS + colour < UNITS))
            def _():
                if depth > 0:
                    for direction in range(2):
                        hop(colour, depth - 1, chunk, direction, True).wait_recv()
                if depth < STAGES:
                    for direction in range(2):
                        hop(colour, depth, chunk, direction, False).start()

    def rows_of(s):
        return pl.ds(pl.multiple_of(s * LENGTH, LENGTH), LENGTH)

    def squares():
        def one(s, _):
            part = x[rows_of(s), :].astype(F32)
            total = jnp.sum(part * part, axis=1, keepdims=True)
            sq[tp, rows_of(s), :] = jnp.broadcast_to(total, (LENGTH, LANES))
            return 0

        lax.fori_loop(0, SEQS, one, 0)

    def pool(s):
        total = sq[0, rows_of(s), :] + sq[1, rows_of(s), :]
        scale = lax.rsqrt(total / WIDTH + EPS)[:, :1]
        at = lax.broadcasted_iota(jnp.int32, (LENGTH, LENGTH), 0)
        col = lax.broadcasted_iota(jnp.int32, (LENGTH, LENGTH), 1)
        for g in range(2):
            reach = jnp.where(tp == 0, 1 << g, 4 << g)
            lower = jnp.maximum(at - reach, 0)
            upper = jnp.minimum(at + reach, LENGTH)
            band = jnp.where((col >= lower) & (col < upper), 1.0, 0.0).astype(BF16)
            count = (upper[:, :1] - lower[:, :1]).astype(F32)
            columns = slice(g * 512, (g + 1) * 512)
            piece = x[rows_of(s), columns].astype(F32) * scale * prm[tp, 0:1, columns]
            piece = piece.astype(BF16)
            window = jnp.dot(band, piece, preferred_element_type=F32)
            mixed[rows_of(s), columns] = (window / count - piece.astype(F32)).astype(BF16)

    def group(s):
        for g in range(2):
            columns = slice(g * 512, (g + 1) * 512)
            maps = w[U_POOL + g].reshape(32, 4, 16, LANES)
            right = jnp.concatenate([maps[:, ct].reshape(512, LANES) for ct in range(4)], axis=1)
            out = dot_nt(mixed[rows_of(s), columns], right) * prm[tp, 4:5, columns]
            mixed[rows_of(s), columns] = out.astype(BF16)

    def project(side, block, dst):
        right = jnp.concatenate(
            [w[U_OUT + k, side, block].reshape(256, LANES) for k in range(8)], axis=1
        )
        columns = pl.ds(pl.multiple_of(block * 256, 256), 256)

        def one(s, _):
            dst[rows_of(s), columns] = dot_nt(mixed[rows_of(s), :], right).astype(BF16)
            return 0

        lax.fori_loop(0, SEQS, one, 0)

    def give_piece(block, index):
        columns = pl.ds(pl.multiple_of(block * 256, 256), 256)
        return across(give.at[:, columns], got.at[:, columns], index + block)

    def middle(s):
        total = own[rows_of(s), :].astype(F32) + got[rows_of(s), :].astype(F32)
        value = x[rows_of(s), :].astype(F32) + total * prm[tp, 1:2, :]
        mid[tp, rows_of(s), :] = value.astype(BF16)

    def mid_piece(s, side):
        ref = mid.at[side, rows_of(s), :]
        return across(ref, ref, 6 + s)

    def norm(s):
        left = mid[0, rows_of(s), :].astype(F32)
        right = mid[1, rows_of(s), :].astype(F32)
        total = jnp.sum(left * left + right * right, axis=1, keepdims=True)
        scale = lax.rsqrt(total / WIDTH + EPS)
        normed[rows_of(s), 0:HALF] = (left * scale * prm[0, 2:3, :]).astype(BF16)
        normed[rows_of(s), HALF:WIDTH] = (right * scale * prm[1, 2:3, :]).astype(BF16)

    def hidden_of(up_raw, gate_raw, columns):
        lifted = (up_raw * ffp[0:1, columns]).astype(BF16).astype(F32)
        at = lax.broadcasted_iota(jnp.int32, lifted.shape, 0)
        before = jnp.where(at == 0, 0.0, pltpu.roll(lifted, 1, 0))
        after = jnp.where(at == LENGTH - 1, 0.0, pltpu.roll(lifted, LENGTH - 1, 0))
        conv = (
            ffp[2:3, columns] * before + ffp[3:4, columns] * lifted + ffp[4:5, columns] * after
        )
        return (jax.nn.gelu(conv) * (gate_raw * ffp[1:2, columns])).astype(BF16)

    def pair(u):
        return jnp.concatenate(
            [w[u].reshape(WIDTH, LANES), w[u + 1].reshape(WIDTH, LANES)], axis=1
        )

    def feed(j, s):
        u = U_FF + 4 * j
        left = normed[rows_of(s), :]
        up_raw = jnp.dot(left, pair(u), preferred_element_type=F32)
        gate_raw = jnp.dot(left, pair(u + 2), preferred_element_type=F32)
        columns = pl.ds(pl.multiple_of(j * 256, 256), 256)
        hid[rows_of(s), columns] = hidden_of(up_raw, gate_raw, columns)

    def feed_last(s):
        both = jnp.dot(normed[rows_of(s), :], pair(U_LAST), preferred_element_type=F32)
        columns = pl.ds(10 * LANES, LANES)
        hid[rows_of(s), columns] = hidden_of(both[:, :LANES], both[:, LANES:], columns)

    def down_part(side, block, tiles):
        return jnp.concatenate(
            [w[U_DOWN + k, side, block].reshape(256, LANES) for k in tiles], axis=1
        )

    def down_first(s):
        def one(n, _):
            right = down_part(n // 4, lax.rem(n, 4), range(8))
            columns = pl.ds(pl.multiple_of(n * 256, 256), 256)
            acc[rows_of(s), columns] = dot_nt(hid[rows_of(s), 0:1024], right)
            return 0

        lax.fori_loop(0, 8, one, 0)

    def down_rest(side, block, dst):
        right = down_part(side, block, range(8, 11))
        wide = pl.ds(pl.multiple_of(side * HALF + block * 256, 256), 256)
        columns = pl.ds(pl.multiple_of(block * 256, 256), 256)

        def one(s, _):
            total = acc[rows_of(s), wide] + dot_nt(hid[rows_of(s), 1024:HID], right)
            dst[rows_of(s), columns] = total.astype(BF16)
            return 0

        lax.fori_loop(0, SEQS, one, 0)

    def compute(m):
        def during(start, count, body):
            @pl.when((m >= start) & (m < start + count))
            def _():
                body(m - start)

        def send_squares(_):
            squares()

        def start_squares(_):
            across(sq.at[tp], sq.at[tp], 1).start()

        def take_squares(_):
            across(sq.at[mate], sq.at[mate], 1).wait_recv()
            across(prm_hbm, prm.at[mate], 0).wait_recv()

        during(0, 1, send_squares)
        during(1, 1, start_squares)
        during(4, 1, take_squares)
        during(4, 4, pool)
        during(23, 4, group)

        def project_out(k):
            for part in range(2):
                project(mate, 2 * k + part, give)
                give_piece(2 * k + part, 2).start()

        def project_own(k):
            for part in range(2):
                project(tp, 2 * k + part, own)

        during(31, 2, project_out)
        during(33, 2, project_own)

        def take_mixer(_):
            for block in range(4):
                give_piece(block, 2).wait_recv()

        def middles(k):
            for part in range(2):
                middle(2 * k + part)
            for part in range(2):
                mid_piece(2 * k + part, tp).start()

        def norms(k):
            for part in range(2):
                mid_piece(2 * k + part, mate).wait_recv()
                norm(2 * k + part)

        during(35, 1, take_mixer)
        during(35, 2, middles)
        during(37, 2, norms)
        during(39, 20, lambda k: feed(k // 4, lax.rem(k, 4)))
        during(59, 4, feed_last)
        during(59, 4, down_first)

    def micro(m, _):
        slot, turn = m // COLOURS, lax.rem(m, COLOURS)
        for colour in range(COLOURS):

            @pl.when(turn == colour)
            def _():
                advance(colour, slot)

        compute(m)
        return 0

    lax.fori_loop(0, SLOTS * COLOURS, micro, 0)

    for block in range(4):
        give_piece(block, 2).wait_send()
    for block in range(4):
        down_rest(mate, block, give)
        give_piece(block, 10).start()
    for block in range(4):
        down_rest(tp, block, own)
    for block in range(4):
        give_piece(block, 10).wait_recv()

    def finish(s, _):
        total = own[rows_of(s), :].astype(F32) + got[rows_of(s), :].astype(F32)
        value = mid[tp, rows_of(s), :].astype(F32) + total * prm[tp, 3:4, :]
        x[rows_of(s), :] = value.astype(BF16)
        return 0

    lax.fori_loop(0, SEQS, finish, 0)
    result = pltpu.make_async_copy(x, y_hbm, y_sem)
    result.start()

    across(prm_hbm, prm.at[tp], 0).wait_send()
    across(sq.at[tp], sq.at[tp], 1).wait_send()
    for s in range(SEQS):
        mid_piece(s, tp).wait_send()
    for block in range(4):
        give_piece(block, 10).wait_send()

    def drain(u, _):
        same_size = normed.at[pl.ds(0, 31 * 32), pl.ds(0, 256)]
        pltpu.make_async_copy(same_size, same_size, send_sem.at[u]).wait()
        return 0

    lax.fori_loop(0, UNITS, drain, 0)
    result.wait()


def layer(
    layer_in,
    mix_gain,
    pool_weight,
    pool_scale,
    out_weight,
    out_scale,
    channel_gain,
    up_weight,
    up_scale,
    gate_weight,
    gate_scale,
    conv_weight,
    down_weight,
    down_scale,
):
    rows = [
        mix_gain.astype(F32),
        out_scale,
        channel_gain.astype(F32),
        down_scale,
        pool_scale.reshape(HALF),
    ]
    prm = jnp.pad(jnp.stack(rows), ((0, 3), (0, 0)))
    ffp = jnp.concatenate(
        [up_scale[None], gate_scale[None], conv_weight, jnp.zeros((3, HID), F32)], axis=0
    )
    anywhere = pl.BlockSpec(memory_space=pl.ANY)
    dma = pltpu.SemaphoreType.DMA
    return pl.pallas_call(
        kernel,
        out_shape=jax.ShapeDtypeStruct((ROWS, HALF), BF16),
        in_specs=[anywhere] * 8,
        out_specs=anywhere,
        scratch_shapes=[
            pltpu.VMEM((UNITS, 2, 4, 4, 64, LANES), BF16),
            pltpu.VMEM((ROWS, HALF), BF16),
            pltpu.VMEM((ROWS, HALF), BF16),
            pltpu.VMEM((ROWS, HALF), BF16),
            pltpu.VMEM((ROWS, HALF), BF16),
            pltpu.VMEM((ROWS, HALF), BF16),
            pltpu.VMEM((2, ROWS, HALF), BF16),
            pltpu.VMEM((ROWS, WIDTH), BF16),
            pltpu.VMEM((ROWS, HID), BF16),
            pltpu.VMEM((ROWS, WIDTH), F32),
            pltpu.VMEM((2, 512, 16), F32),
            pltpu.VMEM((1024, 64), F32),
            pltpu.VMEM((64, HID), F32),
            pltpu.VMEM((64, HID), F32),
            pltpu.VMEM((HID, 64), F32),
            pltpu.VMEM((2, 8, HALF), F32),
            pltpu.VMEM((8, HID), F32),
            pltpu.VMEM((2, ROWS, LANES), F32),
            dma((8,)),
            dma((UNITS,)),
            dma((UNITS, STAGES, 2)),
            dma((14,)),
            dma((14,)),
            dma,
        ],
        compiler_params=pltpu.CompilerParams(
            collective_id=0, has_side_effects=True, vmem_limit_bytes=66_000_000
        ),
    )(layer_in, pool_weight, out_weight, up_weight, gate_weight, down_weight, prm, ffp)


def solution(mesh):
    torus = Mesh(
        mesh.devices.reshape(mesh.shape["rep"], 2, 4, 4, mesh.shape["tp"]),
        ("rep", "fs_0", "fs_1", "fs_2", "tp"),
    )
    in_specs = (
        P(REP_FS, "tp"),
        P("tp"),
        P("tp", None, FS),
        P("tp", None),
        P("tp", FS),
        P("tp"),
        P("tp"),
        P(FS, "tp"),
        P("tp"),
        P(FS, "tp"),
        P("tp"),
        P(None, "tp"),
        P("tp", FS),
        P("tp"),
    )
    out_specs = P(REP_FS, "tp")
    return jax.shard_map(
        layer, mesh=torus, in_specs=in_specs, out_specs=out_specs, check_vma=False
    )
```

time: 512 us -> 143 us (0.28)
  waiting for transfers between devices: 337 us -> 0 us
  Pallas kernels: 0 us -> 127 us
  blocking collectives: 60 us -> 0 us
  matrix products: 39.8 us -> 0 us
  other arithmetic: 20.3 us -> 2.78 us
  local copies, waits for them, and re-layouts: 29.8 us -> 12.5 us
  between operations: 13.6 us -> 0.02 us
  starting transfers between devices: 11.3 us -> 0 us
    all_gather x5 -> x0, waiting for transfers between devices: 336 us -> none  [the longest x2 165 us: side_by_side(): filled = lax.all_gather(both, axis, axis=dim, tiled=True)]
    pallas_call x0 -> x1, Pallas kernels: none -> 127 us  [layer(): pl.pallas_call(kernel, out_shape=jax.ShapeDtypeStruct((ROWS, HALF), BF16)...]
    all_to_all x2 -> x0, blocking collectives: 52.6 us -> none  [summed_on_arrival(): lax.all_to_all(parts, axis, split_axis=0, concat_axis=0, tiled=True)]
    dot_general x7 -> x0, matrix products: 39.8 us -> none  [the longest x1 10.4 us: per_device(): jnp.dot(chan_normed, up_whole, preferred_element_type=jnp.float32)]
    all_to_all x2 -> x0, starting transfers between devices: 11 us -> none  [copy_for_each(): return lax.all_to_all(copies, axis, split_axis=0, concat_axis=0, tiled=True)]
    convert_element_type x12 -> x0, other arithmetic: 8.13 us -> none  [the longest x1 2.22 us: per_device(): return (m32 + chan_sum * down_scale[None]).astype(jnp.bfloat16)]
    all_gather x1 -> x0, blocking collectives: 7.37 us -> none  [stacked_from(): parts = lax.all_gather(parts, axes[k], axis=0, tiled=True)]
    transpose x1 -> x0, local copies, waits for them, and re-layouts: 5.71 us -> none  [stacked_from(): parts.transpose(*turned, *range(len(turns), parts.ndim))]
  transfers between devices with their start and end apart: 7 -> 0, of which waited for: 6 -> 0; matrix products, arithmetic and copies ran while one was open for 10% -> 0% of each run, Pallas kernels for 0% -> 0%
where the time goes in v1:
time: 143 us; the launch traced here: 142 us
  Pallas kernels  127 us (89%)
  local copies, waits for them, and re-layouts  12.5 us (9%)
  other arithmetic  2.78 us (2%)
    pallas_call x1, Pallas kernels, layer(): pl.pallas_call(kernel, out_shape=jax.ShapeDtypeStruct((ROWS, HALF), BF16)...  127 us
    unnamed x5, local copies, waits for them, and re-layouts  9.69 us

profile of v1, /device:TPU:1, one launch (start us, length us, event | category | flops | bytes accessed | tf_op | source)
XLA Modules:
  0.0 142.1 jit_solution(18434332214270043048)
XLA Ops:
  0.0 0.1 pad.8.clone
  0.1 0.7 stack.28
  0.8 0.7 copy.18
  1.5 0.7 stack.29
  2.1 0.7 broadcast_in_dim.9
  2.8 0.7 broadcast_in_dim.10
  3.5 0.7 stack.27
  4.3 0.6 pad.4.prm_hbm
  4.9 1.4 maximum_maximum_fusion.ffp_hbm
  6.3 1.8 %copy.15.pool_hbm = f32[2,512,16]{2,1,0:T(8,128)} copy(f32[2,512,16]{1,2,0:T(8,128)} %param.16) | data formatting | bytes 131072 | tf_op args[2]
  8.2 2.0 %copy.16.out_hbm = f32[1024,64]{1,0:T(8,128)} copy(f32[1024,64]{0,1:T(8,128)} %param.18) | data formatting | bytes 524288 | tf_op args[4]
  10.1 2.1 %copy.17.down_hbm = f32[1408,64]{1,0:T(8,128)} copy(f32[1408,64]{0,1:T(8,128)} %param.26) | data formatting | bytes 720896 | tf_op args[12]
  12.2 126.8 %shard_map.136 = bf16[1024,1024]{1,0:T(8,128)(2,1)} custom-call(bf16[1024,1024]{1,0:T(8,128)(2,1)} %x_hbm.1, f32[2,512,16]{2,1,0:T(8,128)} %copy.15.pool_hbm, f32[1024,64]{1,0:T(8,128)} %copy.16.out_hbm, f32[64,1408]{1,0:T(8,128)} %up_hbm.1, f32[64,1408]{1,0:T(8,128)} %gate_hbm.1, f32[1408,64]{1,0:T(8,128)} %copy.17.down_hbm, f32[8,1024]{1,0:T(8,128)} %pad.4.prm_hbm, ...), custom_call_target="tpu_custom_call" | custom-call | tf_op jit(solution)/shard_map/pallas_call | solution.py:481
  139.0 3.1 %copy.20 = bf16[1024,1024]{1,0:T(8,128)(2,1)} copy(bf16[1024,1024]{1,0:T(8,128)(2,1)} %shard_map.136) | data formatting | bytes 4194304
  (1 shorter events, 0.0 us)

commit v2 on v1

--- a/solution.py
+++ b/solution.py
@@ -56,8 +56,14 @@
     up_hbm,
     gate_hbm,
     down_hbm,
-    prm_hbm,
-    ffp_hbm,
+    mix_gain_hbm,
+    pool_scale_hbm,
+    out_scale_hbm,
+    gain_hbm,
+    up_scale_hbm,
+    gate_scale_hbm,
+    conv_hbm,
+    down_scale_hbm,
     y_hbm,
     w,
     x,
@@ -74,8 +80,15 @@
     st_up,
     st_gate,
     st_down,
-    prm,
-    ffp,
+    mix_gain,
+    pool_scale,
+    out_scale,
+    gain,
+    mate_gain,
+    up_scale,
+    gate_scale,
+    conv_taps,
+    down_scale,
     sq,
     in_sem,
     send_sem,
@@ -113,8 +126,14 @@
                 (gate_hbm, st_gate),
                 (down_hbm, st_down),
                 (x_hbm, x),
-                (prm_hbm, prm.at[tp]),
-                (ffp_hbm, ffp),
+                (mix_gain_hbm, mix_gain),
+                (pool_scale_hbm, pool_scale),
+                (out_scale_hbm, out_scale),
+                (gain_hbm, gain),
+                (up_scale_hbm, up_scale),
+                (gate_scale_hbm, gate_scale),
+                (conv_hbm, conv_taps),
+                (down_scale_hbm, down_scale),
             )
         )
     ]
@@ -131,12 +150,12 @@
     mine = (me["z"], me["y"], me["x"])
     for g in range(2):
         for ct in range(4):
-            block = st_pool[g, ct * LANES : (ct + 1) * LANES, :]
-            w[(U_POOL + g, *mine, pl.ds(ct * 16, 16), slice(None))] = block.T.astype(BF16)
+            block = st_pool[g, :, ct * LANES : (ct + 1) * LANES]
+            w[(U_POOL + g, *mine, pl.ds(ct * 16, 16), slice(None))] = block.astype(BF16)
     for k in range(8):
-        w[(U_OUT + k, *mine)] = st_out[k * LANES : (k + 1) * LANES, :].T.astype(BF16)
+        w[(U_OUT + k, *mine)] = st_out[:, k * LANES : (k + 1) * LANES].astype(BF16)
     for k in range(11):
-        w[(U_DOWN + k, *mine)] = st_down[k * LANES : (k + 1) * LANES, :].T.astype(BF16)
+        w[(U_DOWN + k, *mine)] = st_down[:, k * LANES : (k + 1) * LANES].astype(BF16)
         columns = slice(k * LANES, (k + 1) * LANES)
         at_up = U_LAST if k == 10 else U_FF + 4 * (k // 2) + k % 2
         at_gate = U_LAST + 1 if k == 10 else U_FF + 4 * (k // 2) + 2 + k % 2
@@ -155,7 +174,7 @@
             device_id_type=MESH,
         )
 
-    across(prm_hbm, prm.at[tp], 0).start()
+    across(gain_hbm, mate_gain, 0).start()
 
     def region(u, order, phase, place, rows):
         picks = {}
@@ -220,6 +239,9 @@
                     for direction in range(2):
                         hop(colour, depth, chunk, direction, False).start()
 
+    def row(ref):
+        return ref[...].astype(F32).reshape(1, ref.shape[0])
+
     def rows_of(s):
         return pl.ds(pl.multiple_of(s * LENGTH, LENGTH), LENGTH)
 
@@ -244,7 +266,7 @@
             band = jnp.where((col >= lower) & (col < upper), 1.0, 0.0).astype(BF16)
             count = (upper[:, :1] - lower[:, :1]).astype(F32)
             columns = slice(g * 512, (g + 1) * 512)
-            piece = x[rows_of(s), columns].astype(F32) * scale * prm[tp, 0:1, columns]
+            piece = x[rows_of(s), columns].astype(F32) * scale * row(mix_gain)[:, columns]
             piece = piece.astype(BF16)
             window = jnp.dot(band, piece, preferred_element_type=F32)
             mixed[rows_of(s), columns] = (window / count - piece.astype(F32)).astype(BF16)
@@ -254,7 +276,7 @@
             columns = slice(g * 512, (g + 1) * 512)
             maps = w[U_POOL + g].reshape(32, 4, 16, LANES)
             right = jnp.concatenate([maps[:, ct].reshape(512, LANES) for ct in range(4)], axis=1)
-            out = dot_nt(mixed[rows_of(s), columns], right) * prm[tp, 4:5, columns]
+            out = dot_nt(mixed[rows_of(s), columns], right) * pool_scale[g : g + 1, :]
             mixed[rows_of(s), columns] = out.astype(BF16)
 
     def project(side, block, dst):
@@ -275,7 +297,7 @@
 
     def middle(s):
         total = own[rows_of(s), :].astype(F32) + got[rows_of(s), :].astype(F32)
-        value = x[rows_of(s), :].astype(F32) + total * prm[tp, 1:2, :]
+        value = x[rows_of(s), :].astype(F32) + total * row(out_scale)
         mid[tp, rows_of(s), :] = value.astype(BF16)
 
     def mid_piece(s, side):
@@ -287,18 +309,22 @@
         right = mid[1, rows_of(s), :].astype(F32)
         total = jnp.sum(left * left + right * right, axis=1, keepdims=True)
         scale = lax.rsqrt(total / WIDTH + EPS)
-        normed[rows_of(s), 0:HALF] = (left * scale * prm[0, 2:3, :]).astype(BF16)
-        normed[rows_of(s), HALF:WIDTH] = (right * scale * prm[1, 2:3, :]).astype(BF16)
+        ours, theirs = row(gain), row(mate_gain)
+        left_gain = jnp.where(tp == 0, ours, theirs)
+        right_gain = jnp.where(tp == 0, theirs, ours)
+        normed[rows_of(s), 0:HALF] = (left * scale * left_gain).astype(BF16)
+        normed[rows_of(s), HALF:WIDTH] = (right * scale * right_gain).astype(BF16)
 
     def hidden_of(up_raw, gate_raw, columns):
-        lifted = (up_raw * ffp[0:1, columns]).astype(BF16).astype(F32)
+        taps = conv_taps[:, columns]
+        ups = up_scale[columns].reshape(1, -1)
+        gates = gate_scale[columns].reshape(1, -1)
+        lifted = (up_raw * ups).astype(BF16).astype(F32)
         at = lax.broadcasted_iota(jnp.int32, lifted.shape, 0)
         before = jnp.where(at == 0, 0.0, pltpu.roll(lifted, 1, 0))
         after = jnp.where(at == LENGTH - 1, 0.0, pltpu.roll(lifted, LENGTH - 1, 0))
-        conv = (
-            ffp[2:3, columns] * before + ffp[3:4, columns] * lifted + ffp[4:5, columns] * after
-        )
-        return (jax.nn.gelu(conv) * (gate_raw * ffp[1:2, columns])).astype(BF16)
+        conv = taps[0:1] * before + taps[1:2] * lifted + taps[2:3] * after
+        return (jax.nn.gelu(conv) * (gate_raw * gates)).astype(BF16)
 
     def pair(u):
         return jnp.concatenate(
@@ -358,7 +384,7 @@
 
         def take_squares(_):
             across(sq.at[mate], sq.at[mate], 1).wait_recv()
-            across(prm_hbm, prm.at[mate], 0).wait_recv()
+            across(gain_hbm, mate_gain, 0).wait_recv()
 
         during(0, 1, send_squares)
         during(1, 1, start_squares)
@@ -425,7 +451,7 @@
 
     def finish(s, _):
         total = own[rows_of(s), :].astype(F32) + got[rows_of(s), :].astype(F32)
-        value = mid[tp, rows_of(s), :].astype(F32) + total * prm[tp, 3:4, :]
+        value = mid[tp, rows_of(s), :].astype(F32) + total * row(down_scale)
         x[rows_of(s), :] = value.astype(BF16)
         return 0
 
@@ -433,7 +459,7 @@
     result = pltpu.make_async_copy(x, y_hbm, y_sem)
     result.start()
 
-    across(prm_hbm, prm.at[tp], 0).wait_send()
+    across(gain_hbm, mate_gain, 0).wait_send()
     across(sq.at[tp], sq.at[tp], 1).wait_send()
     for s in range(SEQS):
         mid_piece(s, tp).wait_send()
@@ -465,23 +491,12 @@
     down_weight,
     down_scale,
 ):
-    rows = [
-        mix_gain.astype(F32),
-        out_scale,
-        channel_gain.astype(F32),
-        down_scale,
-        pool_scale.reshape(HALF),
-    ]
-    prm = jnp.pad(jnp.stack(rows), ((0, 3), (0, 0)))
-    ffp = jnp.concatenate(
-        [up_scale[None], gate_scale[None], conv_weight, jnp.zeros((3, HID), F32)], axis=0
-    )
     anywhere = pl.BlockSpec(memory_space=pl.ANY)
     dma = pltpu.SemaphoreType.DMA
     return pl.pallas_call(
         kernel,
         out_shape=jax.ShapeDtypeStruct((ROWS, HALF), BF16),
-        in_specs=[anywhere] * 8,
+        in_specs=[anywhere] * 14,
         out_specs=anywhere,
         scratch_shapes=[
             pltpu.VMEM((UNITS, 2, 4, 4, 64, LANES), BF16),
@@ -494,15 +509,22 @@
             pltpu.VMEM((ROWS, WIDTH), BF16),
             pltpu.VMEM((ROWS, HID), BF16),
             pltpu.VMEM((ROWS, WIDTH), F32),
-            pltpu.VMEM((2, 512, 16), F32),
-            pltpu.VMEM((1024, 64), F32),
+            pltpu.VMEM((2, 16, 512), F32),
+            pltpu.VMEM((64, HALF), F32),
             pltpu.VMEM((64, HID), F32),
             pltpu.VMEM((64, HID), F32),
-            pltpu.VMEM((HID, 64), F32),
-            pltpu.VMEM((2, 8, HALF), F32),
-            pltpu.VMEM((8, HID), F32),
+            pltpu.VMEM((64, HID), F32),
+            pltpu.VMEM((HALF,), BF16),
+            pltpu.VMEM((2, 512), F32),
+            pltpu.VMEM((HALF,), F32),
+            pltpu.VMEM((HALF,), BF16),
+            pltpu.VMEM((HALF,), BF16),
+            pltpu.VMEM((HID,), F32),
+            pltpu.VMEM((HID,), F32),
+            pltpu.VMEM((3, HID), F32),
+            pltpu.VMEM((HALF,), F32),
             pltpu.VMEM((2, ROWS, LANES), F32),
-            dma((8,)),
+            dma((14,)),
             dma((UNITS,)),
             dma((UNITS, STAGES, 2)),
             dma((14,)),
@@ -512,7 +534,22 @@
         compiler_params=pltpu.CompilerParams(
             collective_id=0, has_side_effects=True, vmem_limit_bytes=66_000_000
         ),
-    )(layer_in, pool_weight, out_weight, up_weight, gate_weight, down_weight, prm, ffp)
+    )(
+        layer_in,
+        pool_weight.transpose(0, 2, 1),
+        out_weight.T,
+        up_weight,
+        gate_weight,
+        down_weight.T,
+        mix_gain,
+        pool_scale,
+        out_scale,
+        channel_gain,
+        up_scale,
+        gate_scale,
+        conv_weight,
+        down_scale,
+    )
 
 
 def solution(mesh):

time: 143 us -> 131 us (0.916)
  local copies, waits for them, and re-layouts: 12.5 us -> 3.08 us
  other arithmetic: 2.78 us -> 0 us
    unnamed x5 -> x1, local copies, waits for them, and re-layouts: 9.69 us -> 3.08 us
where the time goes in v2:
time: 131 us
  Pallas kernels  128 us (98%)
  local copies, waits for them, and re-layouts  3.08 us (2%)
    pallas_call x1, Pallas kernels, layer(): pl.pallas_call(kernel, out_shape=jax.ShapeDtypeStruct((ROWS, HALF), BF16)...  128 us
    unnamed x1, local copies, waits for them, and re-layouts  3.08 us

profile of v2, /device:TPU:1, one launch (start us, length us, event | category | flops | bytes accessed | tf_op | source)
XLA Modules:
  0.0 131.0 jit_solution(5648391017105233501)
XLA Ops:
  0.0 127.9 %shard_map.136 = bf16[1024,1024]{1,0:T(8,128)(2,1)} custom-call(bf16[1024,1024]{1,0:T(8,128)(2,1)} %x_hbm.1, f32[2,16,512]{2,1,0:T(8,128)} %bitcast.5, f32[64,1024]{1,0:T(8,128)} %bitcast.4, f32[64,1408]{1,0:T(8,128)} %up_hbm.1, f32[64,1408]{1,0:T(8,128)} %gate_hbm.1, f32[64,1408]{1,0:T(8,128)} %bitcast.3, bf16[1024]{0:T(1024)(128)(2,1)} %mix_gain_hbm.1, ...), custom_call_target="tpu_custom_call" | custom-call | tf_op jit(solution)/shard_map/pallas_call | solution.py:496
  127.9 3.1 %copy.16 = bf16[1024,1024]{1,0:T(8,128)(2,1)} copy(bf16[1024,1024]{1,0:T(8,128)(2,1)} %shard_map.136) | data formatting | bytes 4194304

commit v3 on v2

--- a/solution.py
+++ b/solution.py
@@ -30,18 +30,152 @@
 U_FF = 12
 U_DOWN = 32
 UNITS = 43
-COLOURS = 4
-CHUNKS = 11
 STAGES = 5
-SLOTS = CHUNKS + STAGES
-
-ORDERS = (("x", "y", "z"), ("y", "x", "z"), ("x", "z", "y"), ("y", "z", "x"))
-STEPS = (
-    ((0, "a"), (0, "b"), (1, "a"), (1, "b"), (2, "a")),
-    ((0, "a"), (0, "b"), (1, "a"), (1, "b"), (2, "a")),
-    ((0, "a"), (0, "b"), (1, "a"), (2, "a"), (2, "b")),
-    ((0, "a"), (0, "b"), (1, "a"), (2, "a"), (2, "b")),
+
+ORDERS = (
+    "xyz",
+    "xyz",
+    "xyz",
+    "yzx",
+    "yzx",
+    "xyz",
+    "xzy",
+    "xyz",
+    "yzx",
+    "xyz",
+    "xzy",
+    "yxz",
+    "xyz",
+    "xyz",
+    "xyz",
+    "xzy",
+    "xzy",
+    "yxz",
+    "yzx",
+    "yxz",
+    "zxy",
+    "yzx",
+    "xyz",
+    "yxz",
+    "yzx",
+    "xzy",
+    "yxz",
+    "yzx",
+    "xyz",
+    "yxz",
+    "yxz",
+    "zxy",
+    "yzx",
+    "yxz",
+    "yxz",
+    "zxy",
+    "xyz",
+    "zxy",
+    "yxz",
+    "yzx",
+    "yzx",
+    "zxy",
+    "yxz",
 )
+
+SCHEDULE = (
+    (48, 120, 80, 128, 200, 168, 64, 24, 32, 192, 296, 160, 248, 328, 280,),
+    (72, 8, 104, 16, 0, 144, 320, 216, 312, 256,),
+    (
+        40, 152, 56, 232, 96, 1048, 136, 49, 1168, 112, 1296, 1120, 169, 1160, 184, 1064, 121, 1248,
+        1080, 81, 1328, 65, 1024, 297, 1280, 1128, 25, 88, 1032, 1200,
+    ),
+    (1192, 1072, 1144, 1008, 73, 9, 129, 201, 161, 33, 193, 145, 208, 264,),
+    (1320, 1104, 1216, 1016, 1312, 1000, 1256, 105, 17, 1, 249, 321, 217, 313, 240, 257, 272,),
+    (
+        1040, 1152, 1056, 1232, 1096, 1049, 1136, 1169, 1112, 41, 57, 97, 113, 153, 233, 137, 304,
+        336, 50, 170,
+    ),
+    (
+        1121, 1184, 1081, 1065, 1025, 1088, 1297, 1033, 1073, 1193, 1009, 298, 329, 281, 74, 122,
+        82, 1145, 1129, 1201, 130, 1208, 176, 10, 1264, 1321, 224, 1161, 202, 1217, 1105, 1313, 162,
+        1017, 1001, 1240, 288, 66, 1257, 106, 1272, 1249, 250, 1153, 154, 1050, 1041, 26, 1233,
+        1057, 1137, 1097, 1113, 1304, 1170, 34, 1298, 1336, 18, 171, 1122, 194, 1329, 1082, 146,
+        1281, 1074, 75, 1176, 1130, 322, 1224, 185, 1162, 89, 1202, 2, 218, 1288, 1010, 1250, 177,
+        1066, 314, 225, 67, 1026, 11, 258, 1106, 1154, 1034, 107, 1194, 42, 1018, 1146, 1075, 76,
+        155, 1185, 1089, 1322, 19, 234, 1171, 1218, 1177, 58, 1225, 1002, 1314, 172, 1011, 12, 1258,
+        3, 1107, 209, 265, 27, 98, 1067, 108, 1042, 1155, 43, 1019, 1076, 241, 273, 51, 1234, 235,
+        1058, 20, 68, 1003, 1209, 1172, 1265, 1012, 35, 59, 1098, 99, 4, 1043, 1241, 1273, 114,
+        1027, 1108, 1235, 28, 305, 178, 1068, 44, 195, 1051, 52, 1059, 1020, 1099, 299, 1035, 60,
+        36, 1114, 1305, 1004,
+    ),
+    (1028, 1178, 138, 115,),
+    (330, 179, 100, 289, 1052, 186, 123, 1044, 1195, 196, 1036, 156, 1299, 147, 300, 1060, 1115,),
+    (1138, 1330, 1289, 1179, 337, 83,),
+    (116,),
+    (1186, 1100, 139, 187,),
+    (1196, 1123, 90, 124,),
+    (1300, 180,),
+    (1337, 1156, 210, 131,),
+    (1147, 148,),
+    (1139, 1187, 266, 236,),
+    (1083, 84,),
+    (1116,),
+    (1090,),
+    (1124, 91, 226, 323, 140, 1210, 163,),
+    (1180,),
+    (1148,),
+    (1131,),
+    (211, 188,),
+    (1266, 1084, 1091, 1236, 267, 242, 132,),
+    (1226, 219, 227, 203, 92,),
+    (),
+    (1323, 1140, 1211, 1163, 1267, 324, 212, 164, 1132,),
+    (1242, 1188, 1227, 243, 290,),
+    (274, 251, 228,),
+    (1219, 1092, 220,),
+    (1203, 1324, 282, 306, 268, 1164,),
+    (1243, 315, 204,),
+    (1212, 1290, 1274, 291, 331,),
+    (1220, 244,),
+    (1282, 1228, 1251, 275, 338, 1306, 252, 1204,),
+    (1291, 307, 259, 283, 292,),
+    (1268, 1315,),
+    (1275, 276,),
+    (1331, 1244, 1338, 339, 316, 332,),
+    (1252, 1307, 308,),
+    (1292,),
+    (1283, 1259, 260, 284,),
+    (1339, 1332, 340,),
+    (1276, 1316,),
+    (1260, 1284, 1308,),
+    (),
+    (),
+    (1340,),
+    (),
+    (),
+    (),
+    (),
+    (),
+)
+
+PIECES = (
+    ("squares", 1),
+    ("share", 1),
+    ("pool", 4),
+    ("group", 2),
+    ("project", 8),
+    ("middle", 4),
+    ("norm", 4),
+    ("feed", 20),
+    ("last", 2),
+    ("down", 8),
+)
+TOTAL = sum(count for _, count in PIECES)
+
+
+def steps_of(order):
+    steps = []
+    for phase, dim in enumerate(order):
+        steps += [(phase, "a")] if dim == "z" else [(phase, "a"), (phase, "b")]
+    return steps
+
+
 AXIS = {"x": "fs_2", "y": "fs_1"}
 
 
@@ -75,6 +209,7 @@
     normed,
     hid,
     acc,
+    raw,
     st_pool,
     st_out,
     st_up,
@@ -189,9 +324,9 @@
 
     every, first, second = pl.ds(0, 64), pl.ds(0, 32), pl.ds(32, 32)
 
-    def moves(colour, stage):
-        order = ORDERS[colour]
-        phase, step = STEPS[colour][stage]
+    def moves(u, stage):
+        order = ORDERS[u]
+        phase, step = steps_of(order)[stage]
         dim = order[phase]
         if dim == "z":
             there = 1 - zl
@@ -210,13 +345,12 @@
             (ring(dim, 1), second, left, ring(dim, 2), second),
         )
 
-    def hop(colour, stage, chunk, direction, arriving):
-        u = chunk * COLOURS + colour
-        phase, both = moves(colour, stage)
+    def hop(u, stage, direction, arriving):
+        phase, both = moves(u, stage)
         place, rows, peer, from_place, from_rows = both[direction]
         if arriving:
             place, rows = from_place, from_rows
-        ref = region(u, ORDERS[colour], phase, place, rows)
+        ref = region(u, ORDERS[u], phase, place, rows)
         return pltpu.make_async_remote_copy(
             src_ref=ref,
             dst_ref=ref,
@@ -226,18 +360,15 @@
             device_id_type=MESH,
         )
 
-    def advance(colour, slot):
-        for depth in (0, 5, 4, 3, 2, 1):
-            chunk = slot - depth
-
-            @pl.when((chunk >= 0) & (chunk * COLOURS + colour < UNITS))
-            def _():
-                if depth > 0:
-                    for direction in range(2):
-                        hop(colour, depth - 1, chunk, direction, True).wait_recv()
-                if depth < STAGES:
-                    for direction in range(2):
-                        hop(colour, depth, chunk, direction, False).start()
+    def gather(position):
+        for code in SCHEDULE[position]:
+            arriving, (u, stage) = code >= 1000, divmod(code % 1000, 8)
+            for direction in range(2):
+                copy = hop(u, stage, direction, arriving)
+                if arriving:
+                    copy.wait_recv()
+                else:
+                    copy.start()
 
     def row(ref):
         return ref[...].astype(F32).reshape(1, ref.shape[0])
@@ -271,25 +402,19 @@
             window = jnp.dot(band, piece, preferred_element_type=F32)
             mixed[rows_of(s), columns] = (window / count - piece.astype(F32)).astype(BF16)
 
-    def group(s):
-        for g in range(2):
-            columns = slice(g * 512, (g + 1) * 512)
-            maps = w[U_POOL + g].reshape(32, 4, 16, LANES)
-            right = jnp.concatenate([maps[:, ct].reshape(512, LANES) for ct in range(4)], axis=1)
-            out = dot_nt(mixed[rows_of(s), columns], right) * pool_scale[g : g + 1, :]
-            mixed[rows_of(s), columns] = out.astype(BF16)
+    def group(g):
+        columns = pl.ds(pl.multiple_of(g * 512, 512), 512)
+        maps = w[U_POOL + g].reshape(32, 4, 16, LANES)
+        right = jnp.concatenate([maps[:, ct].reshape(512, LANES) for ct in range(4)], axis=1)
+        out = dot_nt(mixed[:, columns], right) * pool_scale[pl.ds(g, 1), :]
+        normed[:, columns] = out.astype(BF16)
 
     def project(side, block, dst):
         right = jnp.concatenate(
             [w[U_OUT + k, side, block].reshape(256, LANES) for k in range(8)], axis=1
         )
         columns = pl.ds(pl.multiple_of(block * 256, 256), 256)
-
-        def one(s, _):
-            dst[rows_of(s), columns] = dot_nt(mixed[rows_of(s), :], right).astype(BF16)
-            return 0
-
-        lax.fori_loop(0, SEQS, one, 0)
+        dst[:, columns] = dot_nt(normed[:, 0:HALF], right).astype(BF16)
 
     def give_piece(block, index):
         columns = pl.ds(pl.multiple_of(block * 256, 256), 256)
@@ -331,133 +456,162 @@
             [w[u].reshape(WIDTH, LANES), w[u + 1].reshape(WIDTH, LANES)], axis=1
         )
 
-    def feed(j, s):
-        u = U_FF + 4 * j
-        left = normed[rows_of(s), :]
-        up_raw = jnp.dot(left, pair(u), preferred_element_type=F32)
-        gate_raw = jnp.dot(left, pair(u + 2), preferred_element_type=F32)
+    def half_of(h):
+        return pl.ds(pl.multiple_of(h * 512, 512), 512)
+
+    def feed_up(j, h):
+        left = normed[half_of(h), :]
+        raw[...] = jnp.dot(left, pair(U_FF + 4 * j), preferred_element_type=F32)
+
+    def feed_gate(j, h):
+        left = normed[half_of(h), :]
+        gate_raw = jnp.dot(left, pair(U_FF + 4 * j + 2), preferred_element_type=F32)
         columns = pl.ds(pl.multiple_of(j * 256, 256), 256)
-        hid[rows_of(s), columns] = hidden_of(up_raw, gate_raw, columns)
-
-    def feed_last(s):
-        both = jnp.dot(normed[rows_of(s), :], pair(U_LAST), preferred_element_type=F32)
+        for q in range(2):
+            part = slice(q * LENGTH, (q + 1) * LENGTH)
+            hid[rows_of(2 * h + q), columns] = hidden_of(raw[part, :], gate_raw[part], columns)
+
+    def feed_last(h):
+        both = jnp.dot(normed[half_of(h), :], pair(U_LAST), preferred_element_type=F32)
         columns = pl.ds(10 * LANES, LANES)
-        hid[rows_of(s), columns] = hidden_of(both[:, :LANES], both[:, LANES:], columns)
+        for q in range(2):
+            part = both[q * LENGTH : (q + 1) * LENGTH]
+            hid[rows_of(2 * h + q), columns] = hidden_of(part[:, :LANES], part[:, LANES:], columns)
 
     def down_part(side, block, tiles):
         return jnp.concatenate(
             [w[U_DOWN + k, side, block].reshape(256, LANES) for k in tiles], axis=1
         )
 
-    def down_first(s):
-        def one(n, _):
-            right = down_part(n // 4, lax.rem(n, 4), range(8))
-            columns = pl.ds(pl.multiple_of(n * 256, 256), 256)
-            acc[rows_of(s), columns] = dot_nt(hid[rows_of(s), 0:1024], right)
-            return 0
-
-        lax.fori_loop(0, 8, one, 0)
+    def down_first(n):
+        right = down_part(n // 4, lax.rem(n, 4), range(8))
+        columns = pl.ds(pl.multiple_of(n * 256, 256), 256)
+        acc[:, columns] = dot_nt(hid[:, 0:1024], right)
 
     def down_rest(side, block, dst):
         right = down_part(side, block, range(8, 11))
         wide = pl.ds(pl.multiple_of(side * HALF + block * 256, 256), 256)
         columns = pl.ds(pl.multiple_of(block * 256, 256), 256)
-
-        def one(s, _):
-            total = acc[rows_of(s), wide] + dot_nt(hid[rows_of(s), 1024:HID], right)
-            dst[rows_of(s), columns] = total.astype(BF16)
-            return 0
-
-        lax.fori_loop(0, SEQS, one, 0)
+        total = acc[:, wide] + dot_nt(hid[:, 1024:HID], right)
+        dst[:, columns] = total.astype(BF16)
 
     def compute(m):
-        def during(start, count, body):
-            @pl.when((m >= start) & (m < start + count))
+        start = 0
+        starts = {}
+        for name, count in PIECES:
+            starts[name] = (start, count)
+            start += count
+
+        def during(name, body):
+            first_one, count = starts[name]
+
+            @pl.when((m >= first_one) & (m < first_one + count))
             def _():
-                body(m - start)
-
-        def send_squares(_):
-            squares()
-
-        def start_squares(_):
+                body(m - first_one)
+
+        def share(_):
             across(sq.at[tp], sq.at[tp], 1).start()
 
-        def take_squares(_):
-            across(sq.at[mate], sq.at[mate], 1).wait_recv()
-            across(gain_hbm, mate_gain, 0).wait_recv()
-
-        during(0, 1, send_squares)
-        during(1, 1, start_squares)
-        during(4, 1, take_squares)
-        during(4, 4, pool)
-        during(23, 4, group)
-
-        def project_out(k):
-            for part in range(2):
-                project(mate, 2 * k + part, give)
-                give_piece(2 * k + part, 2).start()
-
-        def project_own(k):
-            for part in range(2):
-                project(tp, 2 * k + part, own)
-
-        during(31, 2, project_out)
-        during(33, 2, project_own)
-
-        def take_mixer(_):
-            for block in range(4):
-                give_piece(block, 2).wait_recv()
-
-        def middles(k):
-            for part in range(2):
-                middle(2 * k + part)
-            for part in range(2):
-                mid_piece(2 * k + part, tp).start()
-
-        def norms(k):
-            for part in range(2):
-                mid_piece(2 * k + part, mate).wait_recv()
-                norm(2 * k + part)
-
-        during(35, 1, take_mixer)
-        during(35, 2, middles)
-        during(37, 2, norms)
-        during(39, 20, lambda k: feed(k // 4, lax.rem(k, 4)))
-        during(59, 4, feed_last)
-        during(59, 4, down_first)
+        def pooling(s):
+            @pl.when(s == 0)
+            def _():
+                across(sq.at[mate], sq.at[mate], 1).wait_recv()
+                across(gain_hbm, mate_gain, 0).wait_recv()
+
+            pool(s)
+
+        def projecting(k):
+            @pl.when(k < 4)
+            def _():
+                project(mate, k, give)
+                give_piece(k, 2).start()
+
+            @pl.when(k >= 4)
+            def _():
+                project(tp, k - 4, own)
+
+        def middling(s):
+            @pl.when(s == 0)
+            def _():
+                for block in range(4):
+                    give_piece(block, 2).wait_recv()
+
+            middle(s)
+            mid_piece(s, tp).start()
+
+        def norming(s):
+            mid_piece(s, mate).wait_recv()
+            norm(s)
+
+        def feeding(k):
+            j, h = k // 4, lax.rem(k, 4) // 2
+
+            @pl.when(lax.rem(k, 2) == 0)
+            def _():
+                feed_up(j, h)
+
+            @pl.when(lax.rem(k, 2) == 1)
+            def _():
+                feed_gate(j, h)
+
+        during("squares", lambda _: squares())
+        during("share", share)
+        during("pool", pooling)
+        during("group", group)
+        during("project", projecting)
+        during("middle", middling)
+        during("norm", norming)
+        during("feed", feeding)
+        during("last", feed_last)
+        during("down", down_first)
 
     def micro(m, _):
-        slot, turn = m // COLOURS, lax.rem(m, COLOURS)
-        for colour in range(COLOURS):
-
-            @pl.when(turn == colour)
-            def _():
-                advance(colour, slot)
-
+        def among(low, high):
+            if high - low == 1:
+                gather(low)
+                return
+            half = (low + high) // 2
+            pl.when(m < half)(lambda: among(low, half))
+            pl.when(m >= half)(lambda: among(half, high))
+
+        among(0, TOTAL)
         compute(m)
         return 0
 
-    lax.fori_loop(0, SLOTS * COLOURS, micro, 0)
+    lax.fori_loop(0, TOTAL, micro, 0)
+    gather(TOTAL)
 
     for block in range(4):
         give_piece(block, 2).wait_send()
-    for block in range(4):
+
+    def first_half(block, _):
         down_rest(mate, block, give)
         give_piece(block, 10).start()
-    for block in range(4):
+        return 0
+
+    lax.fori_loop(0, 4, first_half, 0)
+
+    def result(block):
+        columns = pl.ds(pl.multiple_of(block * 256, 256), 256)
+        return pltpu.make_async_copy(x.at[:, columns], y_hbm.at[:, columns], y_sem.at[block])
+
+    def second_half(block, _):
+        columns = pl.ds(pl.multiple_of(block * 256, 256), 256)
         down_rest(tp, block, own)
-    for block in range(4):
         give_piece(block, 10).wait_recv()
 
-    def finish(s, _):
-        total = own[rows_of(s), :].astype(F32) + got[rows_of(s), :].astype(F32)
-        value = mid[tp, rows_of(s), :].astype(F32) + total * row(down_scale)
-        x[rows_of(s), :] = value.astype(BF16)
+        def finish(s, _):
+            total = own[rows_of(s), columns].astype(F32) + got[rows_of(s), columns].astype(F32)
+            scale = down_scale[columns].reshape(1, 256)
+            value = mid[tp, rows_of(s), columns].astype(F32) + total * scale
+            x[rows_of(s), columns] = value.astype(BF16)
+            return 0
+
+        lax.fori_loop(0, SEQS, finish, 0)
+        result(block).start()
         return 0
 
-    lax.fori_loop(0, SEQS, finish, 0)
-    result = pltpu.make_async_copy(x, y_hbm, y_sem)
-    result.start()
+    lax.fori_loop(0, 4, second_half, 0)
 
     across(gain_hbm, mate_gain, 0).wait_send()
     across(sq.at[tp], sq.at[tp], 1).wait_send()
@@ -472,7 +626,8 @@
         return 0
 
     lax.fori_loop(0, UNITS, drain, 0)
-    result.wait()
+    for block in range(4):
+        result(block).wait()
 
 
 def layer(
@@ -509,6 +664,7 @@
             pltpu.VMEM((ROWS, WIDTH), BF16),
             pltpu.VMEM((ROWS, HID), BF16),
             pltpu.VMEM((ROWS, WIDTH), F32),
+            pltpu.VMEM((512, 256), F32),
             pltpu.VMEM((2, 16, 512), F32),
             pltpu.VMEM((64, HALF), F32),
             pltpu.VMEM((64, HID), F32),
@@ -529,7 +685,7 @@
             dma((UNITS, STAGES, 2)),
             dma((14,)),
             dma((14,)),
-            dma,
+            dma((4,)),
         ],
         compiler_params=pltpu.CompilerParams(
             collective_id=0, has_side_effects=True, vmem_limit_bytes=66_000_000

time: 131 us -> 111 us (0.85)
  Pallas kernels: 128 us -> 108 us
    pallas_call x1, Pallas kernels: 128 us -> 108 us  [layer(): pl.pallas_call(kernel, out_shape=jax.ShapeDtypeStruct((ROWS, HALF), BF16)...]
where the time goes in v3:
time: 111 us
  Pallas kernels  108 us (97%)
  local copies, waits for them, and re-layouts  3.08 us (3%)
    pallas_call x1, Pallas kernels, layer(): pl.pallas_call(kernel, out_shape=jax.ShapeDtypeStruct((ROWS, HALF), BF16)...  108 us
    unnamed x1, local copies, waits for them, and re-layouts  3.08 us

profile of v3, /device:TPU:1, one launch (start us, length us, event | category | flops | bytes accessed | tf_op | source)
XLA Modules:
  0.0 111.0 jit_solution(10581004407847746582)
XLA Ops:
  0.0 107.9 %shard_map.136 = bf16[1024,1024]{1,0:T(8,128)(2,1)} custom-call(bf16[1024,1024]{1,0:T(8,128)(2,1)} %x_hbm.1, f32[2,16,512]{2,1,0:T(8,128)} %bitcast.5, f32[64,1024]{1,0:T(8,128)} %bitcast.4, f32[64,1408]{1,0:T(8,128)} %up_hbm.1, f32[64,1408]{1,0:T(8,128)} %gate_hbm.1, f32[64,1408]{1,0:T(8,128)} %bitcast.3, bf16[1024]{0:T(1024)(128)(2,1)} %mix_gain_hbm.1, ...), custom_call_target="tpu_custom_call" | custom-call | tf_op jit(solution)/shard_map/pallas_call | solution.py:651
  107.9 3.1 %copy.16 = bf16[1024,1024]{1,0:T(8,128)(2,1)} copy(bf16[1024,1024]{1,0:T(8,128)(2,1)} %shard_map.136) | data formatting | bytes 4194304

commit v4 on v3

v4 whole, which is shorter than its diff:
```python
import jax
import jax.numpy as jnp
from jax import lax
from jax.experimental import pallas as pl
from jax.experimental.pallas import tpu as pltpu
from jax.sharding import Mesh
from jax.sharding import PartitionSpec as P

LENGTH = 256
FS = ("fs_0", "fs_1", "fs_2")
REP_FS = ("rep", "fs_0", "fs_1", "fs_2")
EPS = 1e-06

F32 = jnp.float32
BF16 = jnp.bfloat16
MESH = pl.DeviceIdType.MESH

ROWS = 1024
HALF = 1024
WIDTH = 2048
HID = 1408
SEQS = ROWS // LENGTH
LANES = 128
PAIR = 2 * LANES

U_POOL = 0
U_OUT = 1
U_LAST = 5
U_FF = 6
U_DOWN = 16
U_END = 21
UNITS = 22
STAGES = 5
SEND_GROUP = 3
FIRST_K = 4

ORDERS = (
    "xyz",
    "yzx",
    "xyz",
    "xyz",
    "xyz",
    "yzx",
    "yzx",
    "xyz",
    "xyz",
    "xzy",
    "yzx",
    "yxz",
    "xyz",
    "yzx",
    "xzy",
    "xzy",
    "yxz",
    "yzx",
    "zxy",
    "xyz",
    "yxz",
    "zxy",
)

SCHEDULE = (
    (24, 72, 8, 104, 144, 168,),
    (0, 48, 32, 80, 112, 40, 16, 136, 64, 88, 1144, 1168, 1024, 1008, 25, 9, 120, 128, 1072, 1104,),
    (1000, 1048, 1, 56, 105, 49, 160,),
    (1032, 1080, 1112, 1040, 33, 96, 81, 41,),
    (1016, 1136, 17, 145, 137,),
    (
        1064, 1088, 1025, 1009, 26, 10, 65, 1120, 1128, 73, 1001, 1105, 106, 152, 1049, 1056, 57,
        1033, 1160, 2, 50, 113, 1081, 169, 1096, 1041, 1017, 1137, 97, 121, 82, 1145, 146, 1065,
        1010, 11, 34, 42, 1073, 1152, 1026, 1057, 1106, 74, 1113, 1169, 1097, 1050, 27, 114, 1121,
        1146, 1002, 1082, 3, 122, 107, 1042, 89, 138, 129, 18, 1034, 1074, 1027, 28, 1114, 35, 1011,
        1003, 1122, 1089, 1129, 66, 12, 1138, 4, 1018, 19, 90, 1035, 75, 1107, 108, 1028, 1066,
        1012, 36, 1019, 130, 67, 1090, 161, 58, 153, 1004,
    ),
    (1108, 51,),
    (20, 1075, 76, 1067, 1161, 1130, 1153, 98, 1036, 162, 1058, 68, 59, 83, 1076, 154, 1051, 1020,),
    (1098,),
    (1162, 99,),
    (1059, 115, 60,),
    (52,),
    (),
    (1154,),
    (1068, 91,),
    (1099, 1083, 84, 100, 155, 123, 1052, 131,),
    (1091,),
    (1060, 43,),
    (1115, 92,),
    (1155, 1084,),
    (1131, 116,),
    (1100, 139,),
    (147, 132,),
    (1123,),
    (1043, 1116, 44, 1092,),
    (124, 156,),
    (170, 163,),
    (1139, 1147, 140, 148,),
    (1132, 1044, 1170, 171, 1124,),
    (1163, 164,),
    (1148, 1156, 1140,),
    (),
    (),
    (1171, 172,),
    (),
    (),
    (),
    (),
    (1164, 1172,),
)

PIECES = (
    ("share", 1),
    ("pool", 4),
    ("group", 2),
    ("project", 8),
    ("norm", 4),
    ("feed", 10),
    ("last", 1),
    ("down", 8),
)
TOTAL = sum(count for _, count in PIECES)

AXIS = {"x": "fs_2", "y": "fs_1"}

X_GAIN, X_SCALE, X_INPUT, X_MIXER, X_FINAL = 0, 1, 2, 3, 11


def steps_of(order):
    steps = []
    for phase, dim in enumerate(order):
        steps += [(phase, "a")] if dim == "z" else [(phase, "a"), (phase, "b")]
    return steps


def shards_in(order, stage):
    phase, step = steps_of(order)[stage]
    held = 1
    for dim in order[:phase]:
        held *= 2 if dim == "z" else 4
    return held if order[phase] == "z" or step == "b" else 2 * held


def dot_nt(left, right):
    return lax.dot_general(left, right, (((1,), (1,)), ((), ())), preferred_element_type=F32)


def kernel(
    x_hbm,
    pool_hbm,
    out_hbm,
    up_hbm,
    gate_hbm,
    down_hbm,
    mix_gain_hbm,
    pool_scale_hbm,
    out_scale_hbm,
    gain_hbm,
    up_scale_hbm,
    gate_scale_hbm,
    conv_hbm,
    down_scale_hbm,
    y,
    w,
    w_end,
    x,
    part,
    got,
    end,
    mid,
    normed,
    hid,
    acc,
    raw,
    st_pool,
    st_out,
    st_up,
    st_gate,
    st_down,
    mix_gain,
    pool_scale,
    out_scale,
    mate_out_scale,
    gain,
    mate_gain,
    up_scale,
    gate_scale,
    conv_taps,
    down_scale,
    in_sem,
    send_sem,
    recv_sem,
    tp_send,
    tp_recv,
    y_sem,
):
    rep = lax.axis_index("rep")
    zl = lax.axis_index("fs_0")
    me = {"z": zl, "y": lax.axis_index("fs_1"), "x": lax.axis_index("fs_2")}
    tp = lax.axis_index("tp")
    mate = 1 - tp
    zz = rep * 2 + zl
    z_up = lax.rem(zz + 1, 4)
    z_down = lax.rem(zz + 3, 4)

    def to_z(place):
        return {"rep": place // 2, "fs_0": lax.rem(place, 2)}

    def ring(dim, shift):
        return lax.rem(me[dim] + shift + 4, 4)

    peers = [to_z(z_up), to_z(z_down), {"tp": mate}]
    for dim in ("x", "y"):
        peers += [{AXIS[dim]: ring(dim, 1)}, {AXIS[dim]: ring(dim, -1)}]

    barrier = pltpu.get_barrier_semaphore()
    for peer in peers:
        pl.semaphore_signal(barrier, inc=1, device_id=peer, device_id_type=MESH)

    loads = [
        pltpu.make_async_copy(src, dst, in_sem.at[k])
        for k, (src, dst) in enumerate(
            (
                (pool_hbm, st_pool),
                (out_hbm, st_out),
                (up_hbm, st_up),
                (gate_hbm, st_gate),
                (down_hbm, st_down),
                (x_hbm, x.at[tp]),
                (mix_gain_hbm, mix_gain),
                (pool_scale_hbm, pool_scale),
                (out_scale_hbm, out_scale),
                (gain_hbm, gain),
                (up_scale_hbm, up_scale),
                (gate_scale_hbm, gate_scale),
                (conv_hbm, conv_taps),
                (down_scale_hbm, down_scale),
            )
        )
    ]
    for load in loads:
        load.start()
    for load in loads[:5]:
        load.wait()

    mine = (me["z"], me["y"], me["x"])
    for g in range(2):
        for ct in range(4):
            block = st_pool[g, :, ct * LANES : (ct + 1) * LANES]
            lanes = pl.ds(g * LANES, LANES)
            w[(U_POOL, *mine, pl.ds(ct * 16, 16), lanes)] = block.astype(BF16)
    for k in range(4):
        w[(U_OUT + k, *mine)] = st_out[:, k * PAIR : (k + 1) * PAIR].astype(BF16)
    for k in range(5):
        columns = slice(k * PAIR, (k + 1) * PAIR)
        w[(U_DOWN + k, *mine)] = st_down[:, columns].astype(BF16)
        w[(U_FF + 2 * k, *mine)] = st_up[:, columns].astype(BF16)
        w[(U_FF + 2 * k + 1, *mine)] = st_gate[:, columns].astype(BF16)
    rest = slice(10 * LANES, HID)
    w[(U_LAST, *mine, slice(None), pl.ds(0, LANES))] = st_up[:, rest].astype(BF16)
    w[(U_LAST, *mine, slice(None), pl.ds(LANES, LANES))] = st_gate[:, rest].astype(BF16)
    w_end[mine] = st_down[:, rest].astype(BF16)

    pl.semaphore_wait(barrier, len(peers))

    def across(src, dst, index):
        return pltpu.make_async_remote_copy(
            src_ref=src,
            dst_ref=dst,
            send_sem=tp_send.at[index],
            recv_sem=tp_recv.at[index],
            device_id={"tp": mate},
            device_id_type=MESH,
        )

    def region(u, order, phase, place, rows):
        picks = {}
        for k, dim in enumerate(order):
            if k < phase:
                picks[dim] = slice(None)
            elif k == phase:
                picks[dim] = pl.ds(place, 1)
            else:
                picks[dim] = pl.ds(me[dim], 1)
        where = (picks["z"], picks["y"], picks["x"], rows, slice(None))
        return w_end.at[where] if u == U_END else w.at[(u, *where)]

    every, first, second = pl.ds(0, 64), pl.ds(0, 32), pl.ds(32, 32)

    def moves(u, stage):
        order = ORDERS[u]
        phase, step = steps_of(order)[stage]
        dim = order[phase]
        if dim == "z":
            return phase, ((zl, first, to_z(z_up)), (zl, second, to_z(z_down)))
        right, left = {AXIS[dim]: ring(dim, 1)}, {AXIS[dim]: ring(dim, -1)}
        if step == "a":
            return phase, ((me[dim], every, right), (me[dim], every, left))
        return phase, ((ring(dim, -1), first, right), (ring(dim, 1), second, left))

    def send(u, stage):
        phase, both = moves(u, stage)
        for place, rows, peer in both:
            ref = region(u, ORDERS[u], phase, place, rows)
            pltpu.make_async_remote_copy(
                src_ref=ref,
                dst_ref=ref,
                send_sem=send_sem.at[u // SEND_GROUP],
                recv_sem=recv_sem.at[u, stage],
                device_id=peer,
                device_id_type=MESH,
            ).start()

    def arrived(u, stage):
        count = shards_in(ORDERS[u], stage)
        box = {1: (1, 1, 1), 2: (1, 1, 2), 4: (1, 1, 4), 8: (1, 2, 4), 16: (1, 4, 4)}[count]
        where = tuple(pl.ds(0, size) for size in box)
        ref = w_end.at[where] if u == U_END else w.at[(u, *where)]
        pltpu.make_async_copy(ref, ref, recv_sem.at[u, stage]).wait()

    def gather(position):
        for code in SCHEDULE[position]:
            u, stage = divmod(code % 1000, 8)
            (arrived if code >= 1000 else send)(u, stage)

    def row(ref):
        return ref[...].astype(F32).reshape(1, ref.shape[0])

    def rows_of(s):
        return pl.ds(pl.multiple_of(s * LENGTH, LENGTH), LENGTH)

    def block_of(n):
        return pl.ds(pl.multiple_of(n * PAIR, PAIR), PAIR)

    mixed = hid

    def pool(s):
        total = jnp.zeros((LENGTH, 1), F32)
        for side in range(2):
            values = x[side, rows_of(s), :].astype(F32)
            total = total + jnp.sum(values * values, axis=1, keepdims=True)
        scale = lax.rsqrt(total / WIDTH + EPS)
        at = lax.broadcasted_iota(jnp.int32, (LENGTH, LENGTH), 0)
        col = lax.broadcasted_iota(jnp.int32, (LENGTH, LENGTH), 1)
        for g in range(2):
            reach = jnp.where(tp == 0, 1 << g, 4 << g)
            lower = jnp.maximum(at - reach, 0)
            upper = jnp.minimum(at + reach, LENGTH)
            band = jnp.where((col >= lower) & (col < upper), 1.0, 0.0).astype(BF16)
            count = (upper[:, :1] - lower[:, :1]).astype(F32)
            columns = slice(g * 512, (g + 1) * 512)
            piece = x[tp, rows_of(s), columns].astype(F32) * scale * row(mix_gain)[:, columns]
            piece = piece.astype(BF16)
            window = jnp.dot(band, piece, preferred_element_type=F32)
            mixed[rows_of(s), columns] = (window / count - piece.astype(F32)).astype(BF16)

    def group(g):
        columns = pl.ds(pl.multiple_of(g * 512, 512), 512)
        lanes = pl.ds(pl.multiple_of(g * LANES, LANES), LANES)
        maps = w[U_POOL, :, :, :, :, lanes].reshape(32, 4, 16, LANES)
        right = jnp.concatenate([maps[:, ct].reshape(512, LANES) for ct in range(4)], axis=1)
        out = dot_nt(mixed[:, columns], right) * pool_scale[pl.ds(g, 1), :]
        normed[:, columns] = out.astype(BF16)

    def project(side, block):
        right = jnp.concatenate(
            [w[U_OUT + k, side, block].reshape(256, PAIR) for k in range(4)], axis=1
        )
        part[side, :, block_of(block)] = dot_nt(normed[:, 0:HALF], right).astype(BF16)

    def mixer_piece(side, block):
        columns = block_of(block)
        index = X_MIXER + side * 4 + block
        return across(part.at[side, :, columns], got.at[side, :, columns], index)

    def final_piece(block):
        columns = block_of(block)
        return across(part.at[mate, :, columns], end.at[:, columns], X_FINAL + block)

    def norm(s):
        ours, theirs = row(gain), row(mate_gain)
        gains = (jnp.where(tp == 0, ours, theirs), jnp.where(tp == 0, theirs, ours))
        ours, theirs = row(out_scale), row(mate_out_scale)
        scales = (jnp.where(tp == 0, ours, theirs), jnp.where(tp == 0, theirs, ours))
        total = jnp.zeros((LENGTH, 1), F32)
        for side in range(2):
            added = part[side, rows_of(s), :].astype(F32) + got[side, rows_of(s), :].astype(F32)
            value = x[side, rows_of(s), :].astype(F32) + added * scales[side]
            value = value.astype(BF16)
            mid[side, rows_of(s), :] = value
            value = value.astype(F32)
            total = total + jnp.sum(value * value, axis=1, keepdims=True)
        scale = lax.rsqrt(total / WIDTH + EPS)
        for side in range(2):
            value = mid[side, rows_of(s), :].astype(F32) * scale * gains[side]
            normed[rows_of(s), side * HALF : (side + 1) * HALF] = value.astype(BF16)

    def hidden_of(up_raw, gate_raw, columns):
        taps = conv_taps[:, columns]
        ups = up_scale[columns].reshape(1, -1)
        gates = gate_scale[columns].reshape(1, -1)
        lifted = (up_raw * ups).astype(BF16).astype(F32)
        at = lax.broadcasted_iota(jnp.int32, lifted.shape, 0)
        before = jnp.where(at == 0, 0.0, pltpu.roll(lifted, 1, 0))
        after = jnp.where(at == LENGTH - 1, 0.0, pltpu.roll(lifted, LENGTH - 1, 0))
        conv = taps[0:1] * before + taps[1:2] * lifted + taps[2:3] * after
        return (jax.nn.gelu(conv) * (gate_raw * gates)).astype(BF16)

    def slab(u):
        return w[u].reshape(WIDTH, PAIR)

    def feed_up(j):
        raw[...] = jnp.dot(normed[...], slab(U_FF + 2 * j), preferred_element_type=F32)

    def feed_gate(j):
        gate_raw = jnp.dot(normed[...], slab(U_FF + 2 * j + 1), preferred_element_type=F32)
        columns = block_of(j)
        for s in range(SEQS):
            part_rows = slice(s * LENGTH, (s + 1) * LENGTH)
            hid[part_rows, columns] = hidden_of(raw[part_rows, :], gate_raw[part_rows], columns)

    def feed_last(_):
        both = jnp.dot(normed[...], slab(U_LAST), preferred_element_type=F32)
        columns = pl.ds(10 * LANES, LANES)
        for s in range(SEQS):
            some = both[s * LENGTH : (s + 1) * LENGTH]
            hid[s * LENGTH : (s + 1) * LENGTH, columns] = hidden_of(
                some[:, :LANES], some[:, LANES:], columns
            )

    def down_first(n):
        side, block = n // 4, lax.rem(n, 4)
        right = jnp.concatenate(
            [w[U_DOWN + k, side, block].reshape(256, PAIR) for k in range(FIRST_K)], axis=1
        )
        acc[:, block_of(n)] = dot_nt(hid[:, 0 : FIRST_K * PAIR], right)

    def down_rest(side, block):
        right = [w[U_DOWN + k, side, block].reshape(256, PAIR) for k in range(FIRST_K, 5)]
        right = jnp.concatenate(right + [w_end[side, block].reshape(256, LANES)], axis=1)
        total = acc[:, block_of(side * 4 + block)] + dot_nt(hid[:, FIRST_K * PAIR : HID], right)
        part[side, :, block_of(block)] = total.astype(BF16)

    def compute(m):
        start = 0
        starts = {}
        for name, count in PIECES:
            starts[name] = (start, count)
            start += count

        def during(name, body):
            first_one, count = starts[name]

            @pl.when((m >= first_one) & (m < first_one + count))
            def _():
                body(m - first_one)

        def share(_):
            for load in loads[5:]:
                load.wait()
            across(x_hbm, x.at[tp], X_INPUT).start()
            across(gain_hbm, mate_gain, X_GAIN).start()
            across(out_scale_hbm, mate_out_scale, X_SCALE).start()

        def pooling(s):
            @pl.when(s == 0)
            def _():
                across(x_hbm, x.at[mate], X_INPUT).wait_recv()
                across(gain_hbm, mate_gain, X_GAIN).wait_recv()
                across(out_scale_hbm, mate_out_scale, X_SCALE).wait_recv()

            pool(s)

        def projecting(k):
            side = jnp.where(k < 4, mate, tp)
            block = lax.rem(k, 4)
            project(side, block)
            mixer_piece(side, block).start()

        def norming(s):
            @pl.when(s == 0)
            def _():
                for side in (mate, tp):
                    for block in range(4):
                        mixer_piece(side, block).wait_recv()

            norm(s)

        def feeding(k):
            @pl.when(lax.rem(k, 2) == 0)
            def _():
                feed_up(k // 2)

            @pl.when(lax.rem(k, 2) == 1)
            def _():
                feed_gate(k // 2)

        during("share", share)
        during("pool", pooling)
        during("group", group)
        during("project", projecting)
        during("norm", norming)
        during("feed", feeding)
        during("last", feed_last)
        during("down", down_first)

    def micro(m, _):
        def among(low, high):
            if high - low == 1:
                gather(low)
                return
            half = (low + high) // 2
            pl.when(m < half)(lambda: among(low, half))
            pl.when(m >= half)(lambda: among(half, high))

        among(0, TOTAL)
        compute(m)
        return 0

    lax.fori_loop(0, TOTAL, micro, 0)
    gather(TOTAL)

    for side in (mate, tp):
        for block in range(4):
            mixer_piece(side, block).wait_send()

    def first_half(block, _):
        down_rest(mate, block)
        final_piece(block).start()
        return 0

    lax.fori_loop(0, 4, first_half, 0)

    def second_half(block, _):
        columns = block_of(block)
        down_rest(tp, block)
        final_piece(block).wait_recv()

        def finish(s, _):
            total = part[tp, rows_of(s), columns].astype(F32) + end[rows_of(s), columns].astype(F32)
            scale = down_scale[columns].reshape(1, PAIR)
            value = mid[tp, rows_of(s), columns].astype(F32) + total * scale
            x[tp, rows_of(s), columns] = value.astype(BF16)
            return 0

        lax.fori_loop(0, SEQS, finish, 0)
        pltpu.make_async_copy(x.at[tp, :, columns], y.at[:, columns], y_sem.at[block]).start()
        return 0

    lax.fori_loop(0, 4, second_half, 0)

    across(x_hbm, x.at[tp], X_INPUT).wait_send()
    across(gain_hbm, mate_gain, X_GAIN).wait_send()
    across(out_scale_hbm, mate_out_scale, X_SCALE).wait_send()
    for block in range(4):
        final_piece(block).wait_send()
    for k in range(U_END // SEND_GROUP + 1):
        lanes = PAIR if k == U_END // SEND_GROUP else 2 * PAIR * SEND_GROUP
        ref = normed.at[pl.ds(0, 31 * 32), pl.ds(0, lanes)]
        pltpu.make_async_copy(ref, ref, send_sem.at[k]).wait()
    for block in range(4):
        columns = block_of(block)
        pltpu.make_async_copy(x.at[tp, :, columns], y.at[:, columns], y_sem.at[block]).wait()


def layer(
    layer_in,
    mix_gain,
    pool_weight,
    pool_scale,
    out_weight,
    out_scale,
    channel_gain,
    up_weight,
    up_scale,
    gate_weight,
    gate_scale,
    conv_weight,
    down_weight,
    down_scale,
):
    anywhere = pl.BlockSpec(memory_space=pl.ANY)
    dma = pltpu.SemaphoreType.DMA
    return pl.pallas_call(
        kernel,
        out_shape=jax.ShapeDtypeStruct((ROWS, HALF), BF16),
        in_specs=[anywhere] * 14,
        out_specs=anywhere,
        scratch_shapes=[
            pltpu.VMEM((U_END, 2, 4, 4, 64, PAIR), BF16),
            pltpu.VMEM((2, 4, 4, 64, LANES), BF16),
            pltpu.VMEM((2, ROWS, HALF), BF16),
            pltpu.VMEM((2, ROWS, HALF), BF16),
            pltpu.VMEM((2, ROWS, HALF), BF16),
            pltpu.VMEM((ROWS, HALF), BF16),
            pltpu.VMEM((2, ROWS, HALF), BF16),
            pltpu.VMEM((ROWS, WIDTH), BF16),
            pltpu.VMEM((ROWS, HID), BF16),
            pltpu.VMEM((ROWS, WIDTH), F32),
            pltpu.VMEM((ROWS, PAIR), F32),
            pltpu.VMEM((2, 16, 512), F32),
            pltpu.VMEM((64, HALF), F32),
            pltpu.VMEM((64, HID), F32),
            pltpu.VMEM((64, HID), F32),
            pltpu.VMEM((64, HID), F32),
            pltpu.VMEM((HALF,), BF16),
            pltpu.VMEM((2, 512), F32),
            pltpu.VMEM((HALF,), F32),
            pltpu.VMEM((HALF,), F32),
            pltpu.VMEM((HALF,), BF16),
            pltpu.VMEM((HALF,), BF16),
            pltpu.VMEM((HID,), F32),
            pltpu.VMEM((HID,), F32),
            pltpu.VMEM((3, HID), F32),
            pltpu.VMEM((HALF,), F32),
            dma((14,)),
            dma((U_END // SEND_GROUP + 1,)),
            dma((UNITS, STAGES)),
            dma((15,)),
            dma((15,)),
            dma((4,)),
        ],
        compiler_params=pltpu.CompilerParams(
            collective_id=0, has_side_effects=True, vmem_limit_bytes=66_000_000
        ),
    )(
        layer_in,
        pool_weight.transpose(0, 2, 1),
        out_weight.T,
        up_weight,
        gate_weight,
        down_weight.T,
        mix_gain,
        pool_scale,
        out_scale,
        channel_gain,
        up_scale,
        gate_scale,
        conv_weight,
        down_scale,
    )


def solution(mesh):
    torus = Mesh(
        mesh.devices.reshape(mesh.shape["rep"], 2, 4, 4, mesh.shape["tp"]),
        ("rep", "fs_0", "fs_1", "fs_2", "tp"),
    )
    in_specs = (
        P(REP_FS, "tp"),
        P("tp"),
        P("tp", None, FS),
        P("tp", None),
        P("tp", FS),
        P("tp"),
        P("tp"),
        P(FS, "tp"),
        P("tp"),
        P(FS, "tp"),
        P("tp"),
        P(None, "tp"),
        P("tp", FS),
        P("tp"),
    )
    out_specs = P(REP_FS, "tp")
    return jax.shard_map(
        layer, mesh=torus, in_specs=in_specs, out_specs=out_specs, check_vma=False
    )
```

time: 111 us -> 104 us (0.937)
  Pallas kernels: 108 us -> 101 us
    pallas_call x1, Pallas kernels: 108 us -> 101 us  [layer(): pl.pallas_call(kernel, out_shape=jax.ShapeDtypeStruct((ROWS, HALF), BF16)...]
where the time goes in v4:
time: 104 us
  Pallas kernels  101 us (97%)
  local copies, waits for them, and re-layouts  3.08 us (3%)
    pallas_call x1, Pallas kernels, layer(): pl.pallas_call(kernel, out_shape=jax.ShapeDtypeStruct((ROWS, HALF), BF16)...  101 us
    unnamed x1, local copies, waits for them, and re-layouts  3.08 us

profile of v4, /device:TPU:1, one launch (start us, length us, event | category | flops | bytes accessed | tf_op | source)
XLA Modules:
  0.0 104.2 jit_solution(11076896843296504498)
XLA Ops:
  0.0 101.1 %shard_map.136 = bf16[1024,1024]{1,0:T(8,128)(2,1)} custom-call(bf16[1024,1024]{1,0:T(8,128)(2,1)} %x_hbm.1, f32[2,16,512]{2,1,0:T(8,128)} %bitcast.5, f32[64,1024]{1,0:T(8,128)} %bitcast.4, f32[64,1408]{1,0:T(8,128)} %up_hbm.1, f32[64,1408]{1,0:T(8,128)} %gate_hbm.1, f32[64,1408]{1,0:T(8,128)} %bitcast.3, bf16[1024]{0:T(1024)(128)(2,1)} %mix_gain_hbm.1, ...), custom_call_target="tpu_custom_call" | custom-call | tf_op jit(solution)/shard_map/pallas_call | solution.py:583
  101.2 3.1 %copy.16 = bf16[1024,1024]{1,0:T(8,128)(2,1)} copy(bf16[1024,1024]{1,0:T(8,128)(2,1)} %shard_map.136) | data formatting | bytes 4194304

commit v5 on v4

--- a/solution.py
+++ b/solution.py
@@ -28,84 +28,90 @@
 U_LAST = 5
 U_FF = 6
 U_DOWN = 16
-U_END = 21
-UNITS = 22
+U_TILE = 19
+UNITS = 24
+TILES = UNITS - U_TILE
 STAGES = 5
-SEND_GROUP = 3
-FIRST_K = 4
+SEND_GROUP = 4
+FIRST = (U_TILE - U_DOWN) * PAIR
 
 ORDERS = (
+    "yzx",
     "xyz",
+    "xzy",
+    "xzy",
+    "yxz",
+    "yzx",
+    "xzy",
+    "yxz",
     "yzx",
     "xyz",
     "xyz",
-    "xyz",
+    "yxz",
+    "yzx",
+    "yxz",
+    "yxz",
+    "xzy",
+    "yxz",
+    "xzy",
+    "xzy",
+    "xzy",
+    "yxz",
     "yzx",
     "yzx",
-    "xyz",
-    "xyz",
-    "xzy",
-    "yzx",
-    "yxz",
-    "xyz",
-    "yzx",
-    "xzy",
-    "xzy",
-    "yxz",
-    "yzx",
-    "zxy",
-    "xyz",
-    "yxz",
-    "zxy",
+    "yxz",
 )
 
 SCHEDULE = (
-    (24, 72, 8, 104, 144, 168,),
-    (0, 48, 32, 80, 112, 40, 16, 136, 64, 88, 1144, 1168, 1024, 1008, 25, 9, 120, 128, 1072, 1104,),
-    (1000, 1048, 1, 56, 105, 49, 160,),
-    (1032, 1080, 1112, 1040, 33, 96, 81, 41,),
-    (1016, 1136, 17, 145, 137,),
+    (16, 24, 48, 32, 128, 0,),
     (
-        1064, 1088, 1025, 1009, 26, 10, 65, 1120, 1128, 73, 1001, 1105, 106, 152, 1049, 1056, 57,
-        1033, 1160, 2, 50, 113, 1081, 169, 1096, 1041, 1017, 1137, 97, 121, 82, 1145, 146, 1065,
-        1010, 11, 34, 42, 1073, 1152, 1026, 1057, 1106, 74, 1113, 1169, 1097, 1050, 27, 114, 1121,
-        1146, 1002, 1082, 3, 122, 107, 1042, 89, 138, 129, 18, 1034, 1074, 1027, 28, 1114, 35, 1011,
-        1003, 1122, 1089, 1129, 66, 12, 1138, 4, 1018, 19, 90, 1035, 75, 1107, 108, 1028, 1066,
-        1012, 36, 1019, 130, 67, 1090, 161, 58, 153, 1004,
+        8, 56, 120, 96, 144, 88, 72, 160, 64, 136, 1016, 1032, 33, 17, 104, 1024, 25, 1128, 152,
+        129, 1048, 49, 1000, 1,
     ),
-    (1108, 51,),
-    (20, 1075, 76, 1067, 1161, 1130, 1153, 98, 1036, 162, 1058, 68, 59, 83, 1076, 154, 1051, 1020,),
-    (1098,),
-    (1162, 99,),
-    (1059, 115, 60,),
-    (52,),
+    (1008, 1056, 9, 80, 57, 112,),
+    (1120, 1096, 1144, 121, 145, 97, 184,),
+    (1088, 1160, 1072, 73, 161, 89, 40,),
+    (
+        1064, 1136, 1033, 1017, 137, 34, 65, 176, 168, 18, 1025, 1104, 26, 105, 1152, 1129, 1049,
+        1001, 1009, 10, 1057, 2, 58, 1080, 1112, 1121, 1097, 1145, 1184, 1161, 122, 1073, 1089,
+        1137, 74, 1040, 1065, 50, 90, 1176, 1018, 1168, 1105, 146, 1026, 1034, 41, 19, 98, 35, 1002,
+        1010, 138, 3, 1122, 1058, 66, 1050, 1074, 1041, 42, 1146, 1090, 75, 1098, 1035, 36, 11, 59,
+        1138, 27, 81, 1066, 91, 1019, 1042, 153, 106, 1075, 76, 1003, 1011, 1059, 4, 1081, 185, 20,
+        1091, 1153, 1036, 99, 82, 12, 1106, 1027, 1185, 28, 1004,
+    ),
+    (1020, 1076,),
+    (107, 169, 177, 154, 113, 51, 60, 67, 1082, 1099, 1028, 1169, 1012,),
+    (1177, 1113, 1154, 1107,),
+    (100, 83, 108,),
     (),
-    (1154,),
-    (1068, 91,),
-    (1099, 1083, 84, 100, 155, 123, 1052, 131,),
-    (1091,),
-    (1060, 43,),
-    (1115, 92,),
-    (1155, 1084,),
-    (1131, 116,),
-    (1100, 139,),
-    (147, 132,),
-    (1123,),
-    (1043, 1116, 44, 1092,),
-    (124, 156,),
-    (170, 163,),
-    (1139, 1147, 140, 148,),
-    (1132, 1044, 1170, 171, 1124,),
-    (1163, 164,),
-    (1148, 1156, 1140,),
+    (139,),
+    (114,),
+    (),
+    (1051, 1060, 1067,),
+    (92, 68, 1083, 52, 1100,),
+    (130,),
+    (123,),
+    (1108, 1114,),
+    (1139, 115, 84, 162, 1068, 43, 1052,),
+    (147,),
+    (1092, 1130, 1115, 178,),
+    (1162, 170, 116,),
+    (1123, 131, 124, 163, 1084,),
+    (1178, 1170, 186,),
+    (1043, 44, 140,),
+    (1147, 1131, 179, 132,),
+    (1163, 1186, 148, 1124, 1116,),
+    (187, 171, 155,),
+    (1044, 1140, 164,),
+    (1179, 180, 1148, 1187, 188, 1132,),
     (),
     (),
-    (1171, 172,),
+    (1155, 1171, 172, 156,),
+    (1164,),
+    (1180,),
     (),
     (),
-    (),
-    (),
-    (1164, 1172,),
+    (1188, 1172, 1156,),
 )
 
 PIECES = (
@@ -122,7 +128,7 @@
 
 AXIS = {"x": "fs_2", "y": "fs_1"}
 
-X_GAIN, X_SCALE, X_INPUT, X_MIXER, X_FINAL = 0, 1, 2, 3, 11
+X_GAIN, X_SCALE, X_INPUT, X_MIXER, X_FINAL = 0, 1, 2, 3, 4
 
 
 def steps_of(order):
@@ -138,6 +144,10 @@
     for dim in order[:phase]:
         held *= 2 if dim == "z" else 4
     return held if order[phase] == "z" or step == "b" else 2 * held
+
+
+def group_of(u):
+    return -(-U_TILE // SEND_GROUP) if u >= U_TILE else u // SEND_GROUP
 
 
 def dot_nt(left, right):
@@ -161,7 +171,7 @@
     down_scale_hbm,
     y,
     w,
-    w_end,
+    w_tile,
     x,
     part,
     got,
@@ -191,7 +201,6 @@
     recv_sem,
     tp_send,
     tp_recv,
-    y_sem,
 ):
     rep = lax.axis_index("rep")
     zl = lax.axis_index("fs_0")
@@ -237,7 +246,7 @@
             )
         )
     ]
-    for load in loads:
+    for load in loads[:5]:
         load.start()
     for load in loads[:5]:
         load.wait()
@@ -252,13 +261,18 @@
         w[(U_OUT + k, *mine)] = st_out[:, k * PAIR : (k + 1) * PAIR].astype(BF16)
     for k in range(5):
         columns = slice(k * PAIR, (k + 1) * PAIR)
-        w[(U_DOWN + k, *mine)] = st_down[:, columns].astype(BF16)
         w[(U_FF + 2 * k, *mine)] = st_up[:, columns].astype(BF16)
         w[(U_FF + 2 * k + 1, *mine)] = st_gate[:, columns].astype(BF16)
     rest = slice(10 * LANES, HID)
     w[(U_LAST, *mine, slice(None), pl.ds(0, LANES))] = st_up[:, rest].astype(BF16)
     w[(U_LAST, *mine, slice(None), pl.ds(LANES, LANES))] = st_gate[:, rest].astype(BF16)
-    w_end[mine] = st_down[:, rest].astype(BF16)
+    for k in range(U_TILE - U_DOWN):
+        w[(U_DOWN + k, *mine)] = st_down[:, k * PAIR : (k + 1) * PAIR].astype(BF16)
+    for k in range(TILES):
+        columns = slice(FIRST + k * LANES, FIRST + (k + 1) * LANES)
+        w_tile[(k, *mine)] = st_down[:, columns].astype(BF16)
+    for load in loads[5:]:
+        load.start()
 
     pl.semaphore_wait(barrier, len(peers))
 
@@ -282,7 +296,7 @@
             else:
                 picks[dim] = pl.ds(me[dim], 1)
         where = (picks["z"], picks["y"], picks["x"], rows, slice(None))
-        return w_end.at[where] if u == U_END else w.at[(u, *where)]
+        return w_tile.at[(u - U_TILE, *where)] if u >= U_TILE else w.at[(u, *where)]
 
     every, first, second = pl.ds(0, 64), pl.ds(0, 32), pl.ds(32, 32)
 
@@ -304,7 +318,7 @@
             pltpu.make_async_remote_copy(
                 src_ref=ref,
                 dst_ref=ref,
-                send_sem=send_sem.at[u // SEND_GROUP],
+                send_sem=send_sem.at[group_of(u)],
                 recv_sem=recv_sem.at[u, stage],
                 device_id=peer,
                 device_id_type=MESH,
@@ -314,7 +328,7 @@
         count = shards_in(ORDERS[u], stage)
         box = {1: (1, 1, 1), 2: (1, 1, 2), 4: (1, 1, 4), 8: (1, 2, 4), 16: (1, 4, 4)}[count]
         where = tuple(pl.ds(0, size) for size in box)
-        ref = w_end.at[where] if u == U_END else w.at[(u, *where)]
+        ref = w_tile.at[(u - U_TILE, *where)] if u >= U_TILE else w.at[(u, *where)]
         pltpu.make_async_copy(ref, ref, recv_sem.at[u, stage]).wait()
 
     def gather(position):
@@ -369,8 +383,7 @@
 
     def mixer_piece(side, block):
         columns = block_of(block)
-        index = X_MIXER + side * 4 + block
-        return across(part.at[side, :, columns], got.at[side, :, columns], index)
+        return across(part.at[side, :, columns], got.at[side, :, columns], X_MIXER)
 
     def final_piece(block):
         columns = block_of(block)
@@ -394,16 +407,17 @@
             value = mid[side, rows_of(s), :].astype(F32) * scale * gains[side]
             normed[rows_of(s), side * HALF : (side + 1) * HALF] = value.astype(BF16)
 
-    def hidden_of(up_raw, gate_raw, columns):
+    def activation(up_raw, columns):
         taps = conv_taps[:, columns]
         ups = up_scale[columns].reshape(1, -1)
-        gates = gate_scale[columns].reshape(1, -1)
         lifted = (up_raw * ups).astype(BF16).astype(F32)
         at = lax.broadcasted_iota(jnp.int32, lifted.shape, 0)
         before = jnp.where(at == 0, 0.0, pltpu.roll(lifted, 1, 0))
         after = jnp.where(at == LENGTH - 1, 0.0, pltpu.roll(lifted, LENGTH - 1, 0))
-        conv = taps[0:1] * before + taps[1:2] * lifted + taps[2:3] * after
-        return (jax.nn.gelu(conv) * (gate_raw * gates)).astype(BF16)
+        return jax.nn.gelu(taps[0:1] * before + taps[1:2] * lifted + taps[2:3] * after)
+
+    def hidden_of(active, gate_raw, columns):
+        return (active * (gate_raw * gate_scale[columns].reshape(1, -1))).astype(BF16)
 
     def slab(u):
         return w[u].reshape(WIDTH, PAIR)
@@ -412,33 +426,33 @@
         raw[...] = jnp.dot(normed[...], slab(U_FF + 2 * j), preferred_element_type=F32)
 
     def feed_gate(j):
-        gate_raw = jnp.dot(normed[...], slab(U_FF + 2 * j + 1), preferred_element_type=F32)
         columns = block_of(j)
         for s in range(SEQS):
-            part_rows = slice(s * LENGTH, (s + 1) * LENGTH)
-            hid[part_rows, columns] = hidden_of(raw[part_rows, :], gate_raw[part_rows], columns)
+            some = slice(s * LENGTH, (s + 1) * LENGTH)
+            raw[some, :] = activation(raw[some, :], columns)
+        gate_raw = jnp.dot(normed[...], slab(U_FF + 2 * j + 1), preferred_element_type=F32)
+        hid[:, columns] = hidden_of(raw[...], gate_raw, columns)
 
     def feed_last(_):
         both = jnp.dot(normed[...], slab(U_LAST), preferred_element_type=F32)
         columns = pl.ds(10 * LANES, LANES)
         for s in range(SEQS):
-            some = both[s * LENGTH : (s + 1) * LENGTH]
-            hid[s * LENGTH : (s + 1) * LENGTH, columns] = hidden_of(
-                some[:, :LANES], some[:, LANES:], columns
-            )
+            some = slice(s * LENGTH, (s + 1) * LENGTH)
+            active = activation(both[some, :LANES], columns)
+            hid[some, columns] = hidden_of(active, both[some, LANES:], columns)
 
     def down_first(n):
         side, block = n // 4, lax.rem(n, 4)
         right = jnp.concatenate(
-            [w[U_DOWN + k, side, block].reshape(256, PAIR) for k in range(FIRST_K)], axis=1
+            [w[u, side, block].reshape(256, PAIR) for u in range(U_DOWN, U_TILE)], axis=1
         )
-        acc[:, block_of(n)] = dot_nt(hid[:, 0 : FIRST_K * PAIR], right)
+        acc[:, block_of(n)] = dot_nt(hid[:, 0:FIRST], right)
 
     def down_rest(side, block):
-        right = [w[U_DOWN + k, side, block].reshape(256, PAIR) for k in range(FIRST_K, 5)]
-        right = jnp.concatenate(right + [w_end[side, block].reshape(256, LANES)], axis=1)
-        total = acc[:, block_of(side * 4 + block)] + dot_nt(hid[:, FIRST_K * PAIR : HID], right)
-        part[side, :, block_of(block)] = total.astype(BF16)
+        right = jnp.concatenate(
+            [w_tile[k, side, block].reshape(256, LANES) for k in range(TILES)], axis=1
+        )
+        return acc[:, block_of(side * 4 + block)] + dot_nt(hid[:, FIRST:HID], right)
 
     def compute(m):
         start = 0
@@ -479,9 +493,7 @@
         def norming(s):
             @pl.when(s == 0)
             def _():
-                for side in (mate, tp):
-                    for block in range(4):
-                        mixer_piece(side, block).wait_recv()
+                across(part, got, X_MIXER).wait_recv()
 
             norm(s)
 
@@ -519,12 +531,10 @@
     lax.fori_loop(0, TOTAL, micro, 0)
     gather(TOTAL)
 
-    for side in (mate, tp):
-        for block in range(4):
-            mixer_piece(side, block).wait_send()
+    across(part, got, X_MIXER).wait_send()
 
     def first_half(block, _):
-        down_rest(mate, block)
+        part[mate, :, block_of(block)] = down_rest(mate, block).astype(BF16)
         final_piece(block).start()
         return 0
 
@@ -532,18 +542,10 @@
 
     def second_half(block, _):
         columns = block_of(block)
-        down_rest(tp, block)
         final_piece(block).wait_recv()
-
-        def finish(s, _):
-            total = part[tp, rows_of(s), columns].astype(F32) + end[rows_of(s), columns].astype(F32)
-            scale = down_scale[columns].reshape(1, PAIR)
-            value = mid[tp, rows_of(s), columns].astype(F32) + total * scale
-            x[tp, rows_of(s), columns] = value.astype(BF16)
-            return 0
-
-        lax.fori_loop(0, SEQS, finish, 0)
-        pltpu.make_async_copy(x.at[tp, :, columns], y.at[:, columns], y_sem.at[block]).start()
+        total = down_rest(tp, block).astype(BF16).astype(F32) + end[:, columns].astype(F32)
+        scale = down_scale[columns].reshape(1, PAIR)
+        y[:, columns] = (mid[tp, :, columns].astype(F32) + total * scale).astype(BF16)
         return 0
 
     lax.fori_loop(0, 4, second_half, 0)
@@ -553,13 +555,11 @@
     across(out_scale_hbm, mate_out_scale, X_SCALE).wait_send()
     for block in range(4):
         final_piece(block).wait_send()
-    for k in range(U_END // SEND_GROUP + 1):
-        lanes = PAIR if k == U_END // SEND_GROUP else 2 * PAIR * SEND_GROUP
-        ref = normed.at[pl.ds(0, 31 * 32), pl.ds(0, lanes)]
+    full, over = divmod(U_TILE, SEND_GROUP)
+    lanes = [2 * PAIR * SEND_GROUP] * full + [2 * PAIR * over, PAIR * TILES]
+    for k in range(full + 2):
+        ref = normed.at[pl.ds(0, 31 * 32), pl.ds(0, lanes[k])]
         pltpu.make_async_copy(ref, ref, send_sem.at[k]).wait()
-    for block in range(4):
-        columns = block_of(block)
-        pltpu.make_async_copy(x.at[tp, :, columns], y.at[:, columns], y_sem.at[block]).wait()
 
 
 def layer(
@@ -582,12 +582,12 @@
     dma = pltpu.SemaphoreType.DMA
     return pl.pallas_call(
         kernel,
-        out_shape=jax.ShapeDtypeStruct((ROWS, HALF), BF16),
+        out_shape=pltpu.VMEM((ROWS, HALF), BF16),
         in_specs=[anywhere] * 14,
-        out_specs=anywhere,
+        out_specs=pl.BlockSpec(memory_space=pltpu.VMEM),
         scratch_shapes=[
-            pltpu.VMEM((U_END, 2, 4, 4, 64, PAIR), BF16),
-            pltpu.VMEM((2, 4, 4, 64, LANES), BF16),
+            pltpu.VMEM((U_TILE, 2, 4, 4, 64, PAIR), BF16),
+            pltpu.VMEM((TILES, 2, 4, 4, 64, LANES), BF16),
             pltpu.VMEM((2, ROWS, HALF), BF16),
             pltpu.VMEM((2, ROWS, HALF), BF16),
             pltpu.VMEM((2, ROWS, HALF), BF16),
@@ -613,14 +613,13 @@
             pltpu.VMEM((3, HID), F32),
             pltpu.VMEM((HALF,), F32),
             dma((14,)),
-            dma((U_END // SEND_GROUP + 1,)),
+            dma((group_of(U_TILE) + 1,)),
             dma((UNITS, STAGES)),
-            dma((15,)),
-            dma((15,)),
-            dma((4,)),
+            dma((8,)),
+            dma((8,)),
         ],
         compiler_params=pltpu.CompilerParams(
-            collective_id=0, has_side_effects=True, vmem_limit_bytes=66_000_000
+            collective_id=0, has_side_effects=True, vmem_limit_bytes=63_500_000
         ),
     )(
         layer_in,

time: 104 us -> 101 us (0.971)
  local copies, waits for them, and re-layouts: 3.08 us -> 1.32 us
    unnamed x1, local copies, waits for them, and re-layouts: 3.08 us -> 1.32 us
    pallas_call x1, Pallas kernels: 101 us -> 100 us  [layer(): pl.pallas_call(kernel, out_shape=pltpu.VMEM((ROWS, HALF), BF16), in_specs...]
where the time goes in v5:
time: 101 us
  Pallas kernels  100 us (99%)
  local copies, waits for them, and re-layouts  1.32 us (1%)
    pallas_call x1, Pallas kernels, layer(): pl.pallas_call(kernel, out_shape=pltpu.VMEM((ROWS, HALF), BF16), in_specs...  100 us

profile of v5, /device:TPU:1, one launch (start us, length us, event | category | flops | bytes accessed | tf_op | source)
XLA Modules:
  0.0 101.3 jit_solution(11805797027480935906)
XLA Ops:
  0.0 100.0 %shard_map.136 = bf16[1024,1024]{1,0:T(8,128)(2,1)S(1)} custom-call(bf16[1024,1024]{1,0:T(8,128)(2,1)} %x_hbm.1, f32[2,16,512]{2,1,0:T(8,128)} %bitcast.5, f32[64,1024]{1,0:T(8,128)} %bitcast.4, f32[64,1408]{1,0:T(8,128)} %up_hbm.1, f32[64,1408]{1,0:T(8,128)} %gate_hbm.1, f32[64,1408]{1,0:T(8,128)} %bitcast.3, bf16[1024]{0:T(1024)(128)(2,1)} %mix_gain_hbm.1, ...), custom_call_target="tpu_custom_call" | custom-call | tf_op jit(solution)/shard_map/pallas_call | solution.py:583
  100.0 1.3 %copy.16 = bf16[1024,1024]{1,0:T(8,128)(2,1)} copy(bf16[1024,1024]{1,0:T(8,128)(2,1)S(1)} %shard_map.136) | data formatting | bytes 4194304

commit v6 on v5

--- a/solution.py
+++ b/solution.py
@@ -37,81 +37,81 @@
 
 ORDERS = (
     "yzx",
+    "yxz",
+    "yxz",
+    "yxz",
+    "xzy",
+    "yxz",
     "xyz",
     "xzy",
     "xzy",
-    "yxz",
     "yzx",
     "xzy",
-    "yxz",
-    "yzx",
-    "xyz",
-    "xyz",
-    "yxz",
-    "yzx",
-    "yxz",
-    "yxz",
-    "xzy",
-    "yxz",
-    "xzy",
-    "xzy",
-    "xzy",
-    "yxz",
+    "xzy",
+    "yxz",
+    "yxz",
+    "xzy",
     "yzx",
     "yzx",
     "yxz",
+    "xyz",
+    "zyx",
+    "yxz",
+    "yxz",
+    "xzy",
+    "xzy",
 )
 
 SCHEDULE = (
-    (16, 24, 48, 32, 128, 0,),
+    (80, 48, 32, 144, 24, 0, 16, 168, 40, 152,),
     (
-        8, 56, 120, 96, 144, 88, 72, 160, 64, 136, 1016, 1032, 33, 17, 104, 1024, 25, 1128, 152,
-        129, 1048, 49, 1000, 1,
+        112, 8, 56, 96, 88, 72, 184, 1152, 176, 160, 1080, 1024, 81, 25, 64, 128, 1048, 1000, 49, 1,
+        1032, 1016, 33, 17, 1168, 169, 1144, 145, 104,
     ),
-    (1008, 1056, 9, 80, 57, 112,),
-    (1120, 1096, 1144, 121, 145, 97, 184,),
-    (1088, 1160, 1072, 73, 161, 89, 40,),
+    (1040, 1112, 1008, 113, 41, 9,),
+    (1056, 1096, 1088, 89, 57, 97, 136,),
+    (1184, 1072, 1176, 1160, 1081, 1025, 26, 161, 73, 120, 82,),
     (
-        1064, 1136, 1033, 1017, 137, 34, 65, 176, 168, 18, 1025, 1104, 26, 105, 1152, 1129, 1049,
-        1001, 1009, 10, 1057, 2, 58, 1080, 1112, 1121, 1097, 1145, 1184, 1161, 122, 1073, 1089,
-        1137, 74, 1040, 1065, 50, 90, 1176, 1018, 1168, 1105, 146, 1026, 1034, 41, 19, 98, 35, 1002,
-        1010, 138, 3, 1122, 1058, 66, 1050, 1074, 1041, 42, 1146, 1090, 75, 1098, 1035, 36, 11, 59,
-        1138, 27, 81, 1066, 91, 1019, 1042, 153, 106, 1075, 76, 1003, 1011, 1059, 4, 1081, 185, 20,
-        1091, 1153, 1036, 99, 82, 12, 1106, 1027, 1185, 28, 1004,
+        1064, 1128, 1049, 1001, 177, 65, 129, 50, 2, 1033, 34, 185, 1017, 18, 1169, 1145, 1113, 114,
+        1104, 1089, 1041, 1057, 1009, 90, 1097, 146, 1082, 1136, 1161, 10, 1073, 58, 1002, 1120,
+        1026, 1129, 1177, 1065, 130, 1185, 83, 1034, 27, 186, 1114, 66, 1050, 3, 1018, 1090, 74,
+        1058, 178, 1146, 1010, 137, 1130, 121, 35, 1186, 1027, 28, 19, 1066, 11, 1074, 1178, 1083,
+        42, 1137, 1121, 122, 84, 1003, 4, 1019, 20, 147, 1011, 1028, 75, 105, 51, 1035, 1122, 12,
+        36, 1042, 1084, 67, 1004,
     ),
-    (1020, 1076,),
-    (107, 169, 177, 154, 113, 51, 60, 67, 1082, 1099, 1028, 1169, 1012,),
-    (1177, 1113, 1154, 1107,),
-    (100, 83, 108,),
+    (1147, 1105, 43,),
+    (1020, 1051, 138, 52, 1036, 98, 153, 1075, 59, 1043, 1012,),
+    (76, 44,),
     (),
-    (139,),
-    (114,),
-    (),
-    (1051, 1060, 1067,),
-    (92, 68, 1083, 52, 1100,),
-    (130,),
-    (123,),
-    (1108, 1114,),
-    (1139, 115, 84, 162, 1068, 43, 1052,),
-    (147,),
-    (1092, 1130, 1115, 178,),
-    (1162, 170, 116,),
-    (1123, 131, 124, 163, 1084,),
-    (1178, 1170, 186,),
-    (1043, 44, 140,),
-    (1147, 1131, 179, 132,),
-    (1163, 1186, 148, 1124, 1116,),
-    (187, 171, 155,),
-    (1044, 1140, 164,),
-    (1179, 180, 1148, 1187, 188, 1132,),
+    (1138,),
+    (1067, 1153, 139,),
+    (91,),
+    (1098, 99,),
+    (1052, 131, 148,),
+    (1076, 1059, 1139,),
+    (60,),
+    (1099, 1044, 106,),
+    (140,),
+    (68,),
+    (1091, 170,),
+    (1131, 132, 92, 1148, 1060,),
+    (1106, 107, 154, 115, 100, 162, 1068,),
+    (1170, 171,),
+    (1140, 1092, 1132, 1154, 123,),
+    (1107, 187, 108,),
+    (1162, 1171,),
+    (163, 179,),
+    (1100, 155,),
+    (1115, 172,),
+    (116,),
     (),
     (),
-    (1155, 1171, 172, 156,),
-    (1164,),
-    (1180,),
-    (),
-    (),
-    (1188, 1172, 1156,),
+    (1187,),
+    (1123, 124, 188,),
+    (1163, 1108, 164,),
+    (1179, 1155, 156, 180, 1172, 1116,),
+    (1124, 1188,),
+    (1164, 1156, 1180,),
 )
 
 PIECES = (
@@ -120,9 +120,10 @@
     ("group", 2),
     ("project", 8),
     ("norm", 4),
-    ("feed", 10),
     ("last", 1),
+    ("feed", 6),
     ("down", 8),
+    ("feed again", 4),
 )
 TOTAL = sum(count for _, count in PIECES)
 
@@ -511,8 +512,14 @@
         during("group", group)
         during("project", projecting)
         during("norm", norming)
-        during("feed", feeding)
         during("last", feed_last)
+        again = starts["feed again"][0]
+        early, late = (m >= starts["feed"][0]) & (m < starts["down"][0]), m >= again
+
+        @pl.when(early | late)
+        def _():
+            feeding(jnp.where(late, m - again + starts["feed"][1], m - starts["feed"][0]))
+
         during("down", down_first)
 
     def micro(m, _):

time: 101 us -> 99.7 us (0.987)
  Pallas kernels: 100 us -> 98.2 us
    pallas_call x1, Pallas kernels: 100 us -> 98.2 us  [layer(): pl.pallas_call(kernel, out_shape=pltpu.VMEM((ROWS, HALF), BF16), in_specs...]
where the time goes in v6:
time: 99.7 us; the launch traced here: 99.6 us
  Pallas kernels  98.2 us (98%)
  local copies, waits for them, and re-layouts  1.32 us (1%)
    pallas_call x1, Pallas kernels, layer(): pl.pallas_call(kernel, out_shape=pltpu.VMEM((ROWS, HALF), BF16), in_specs...  98.2 us

profile of v6, /device:TPU:1, one launch (start us, length us, event | category | flops | bytes accessed | tf_op | source)
XLA Modules:
  0.0 99.6 jit_solution(7370979650286822218)
XLA Ops:
  0.0 98.2 %shard_map.136 = bf16[1024,1024]{1,0:T(8,128)(2,1)S(1)} custom-call(bf16[1024,1024]{1,0:T(8,128)(2,1)} %x_hbm.1, f32[2,16,512]{2,1,0:T(8,128)} %bitcast.5, f32[64,1024]{1,0:T(8,128)} %bitcast.4, f32[64,1408]{1,0:T(8,128)} %up_hbm.1, f32[64,1408]{1,0:T(8,128)} %gate_hbm.1, f32[64,1408]{1,0:T(8,128)} %bitcast.3, bf16[1024]{0:T(1024)(128)(2,1)} %mix_gain_hbm.1, ...), custom_call_target="tpu_custom_call" | custom-call | tf_op jit(solution)/shard_map/pallas_call | solution.py:590
  98.2 1.3 %copy.16 = bf16[1024,1024]{1,0:T(8,128)(2,1)} copy(bf16[1024,1024]{1,0:T(8,128)(2,1)S(1)} %shard_map.136) | data formatting | bytes 4194304

commit v7 on v6

--- a/solution.py
+++ b/solution.py
@@ -36,88 +36,99 @@
 FIRST = (U_TILE - U_DOWN) * PAIR
 
 ORDERS = (
+    "yxz",
+    "yzx",
+    "xyz",
+    "xzy",
+    "xzy",
+    "yxz",
     "yzx",
     "yxz",
-    "yxz",
-    "yxz",
+    "xzy",
     "xzy",
     "yxz",
     "xyz",
-    "xzy",
-    "xzy",
-    "yzx",
-    "xzy",
-    "xzy",
-    "yxz",
-    "yxz",
+    "xyz",
+    "xyz",
     "xzy",
     "yzx",
     "yzx",
     "yxz",
+    "yzx",
+    "xzy",
+    "yxz",
+    "yzx",
     "xyz",
-    "zyx",
-    "yxz",
-    "yxz",
-    "xzy",
-    "xzy",
+    "zxy",
 )
 
 SCHEDULE = (
-    (80, 48, 32, 144, 24, 0, 16, 168, 40, 152,),
+    (32, 24, 0, 40, 184,),
     (
-        112, 8, 56, 96, 88, 72, 184, 1152, 176, 160, 1080, 1024, 81, 25, 64, 128, 1048, 1000, 49, 1,
-        1032, 1016, 33, 17, 1168, 169, 1144, 145, 104,
+        16, 56, 64, 48, 72, 136, 152, 8, 112, 128, 96, 1184, 144, 1032, 1000, 33, 176, 1, 1024,
+        1040, 25, 41, 1016, 1056, 17, 88, 57, 160, 120, 1064, 1048, 1072, 1136, 65, 73, 104, 49,
+        137, 1152, 1008, 1112, 153, 113, 185, 9, 168, 80, 1128, 1096, 1033, 1144, 97, 145, 129, 34,
+        1176, 1001, 2, 1025, 1041, 26, 1017, 18, 1057, 1160, 1088,
     ),
-    (1040, 1112, 1008, 113, 41, 9,),
-    (1056, 1096, 1088, 89, 57, 97, 136,),
-    (1184, 1072, 1176, 1160, 1081, 1025, 26, 161, 73, 120, 82,),
     (
-        1064, 1128, 1049, 1001, 177, 65, 129, 50, 2, 1033, 34, 185, 1017, 18, 1169, 1145, 1113, 114,
-        1104, 1089, 1041, 1057, 1009, 90, 1097, 146, 1082, 1136, 1161, 10, 1073, 58, 1002, 1120,
-        1026, 1129, 1177, 1065, 130, 1185, 83, 1034, 27, 186, 1114, 66, 1050, 3, 1018, 1090, 74,
-        1058, 178, 1146, 1010, 137, 1130, 121, 35, 1186, 1027, 28, 19, 1066, 11, 1074, 1178, 1083,
-        42, 1137, 1121, 122, 84, 1003, 4, 1019, 20, 147, 1011, 1028, 75, 105, 51, 1035, 1122, 12,
-        36, 1042, 1084, 67, 1004,
+        1065, 1120, 66, 1073, 1049, 1137, 42, 1104, 1009, 1153, 121, 1168, 10, 1113, 169, 161, 1080,
+        81,
     ),
-    (1147, 1105, 43,),
-    (1020, 1051, 138, 52, 1036, 98, 153, 1075, 59, 1043, 1012,),
-    (76, 44,),
-    (),
-    (1138,),
-    (1067, 1153, 139,),
-    (91,),
-    (1098, 99,),
-    (1052, 131, 148,),
-    (1076, 1059, 1139,),
-    (60,),
-    (1099, 1044, 106,),
-    (140,),
-    (68,),
-    (1091, 170,),
-    (1131, 132, 92, 1148, 1060,),
-    (1106, 107, 154, 115, 100, 162, 1068,),
-    (1170, 171,),
-    (1140, 1092, 1132, 1154, 123,),
-    (1107, 187, 108,),
-    (1162, 1171,),
-    (163, 179,),
-    (1100, 155,),
-    (1115, 172,),
-    (116,),
-    (),
+    (1185, 1145, 1097, 98, 1129, 146, 1034, 138, 50, 1026, 27,),
+    (1002, 1018, 130, 1066, 1121, 1169, 1161, 3, 1081, 74, 1010, 89,),
+    (
+        1042, 43, 170, 1146, 122, 1098, 11, 1050, 114, 19, 1138, 1130, 154, 35, 1003, 4, 1089, 1074,
+        1170, 1043, 1122, 1027, 139, 1114, 1019, 186, 1154, 58, 28, 20, 1011, 12, 90, 1139, 1186,
+        1035, 1004,
+    ),
+    (82, 36,),
+    (1058, 44, 1028, 59, 75, 51, 1012, 1090, 1020,),
+    (),
+    (),
+    (1082, 140,),
+    (1036,),
+    (),
+    (1059, 91,),
+    (),
+    (83,),
+    (67,),
+    (1044, 177, 105,),
+    (131, 60,),
+    (),
+    (1075,),
+    (1051,),
+    (1091,),
+    (1083, 1177, 76, 1105, 1140,),
+    (52,),
+    (106, 92,),
+    (),
+    (1067, 147,),
+    (1131, 1060, 68, 1076, 84, 99, 1052,),
+    (132, 178,),
+    (1106, 107, 1092, 162, 115, 1068,),
+    (1147, 1099, 148, 100,),
+    (1178, 123, 1132, 1107, 1084,),
+    (1162, 179, 187, 108,),
+    (1148,),
+    (155,),
+    (163,),
+    (1115, 1100, 1179, 171,),
+    (),
+    (116, 180,),
     (),
     (1187,),
-    (1123, 124, 188,),
-    (1163, 1108, 164,),
-    (1179, 1155, 156, 180, 1172, 1116,),
-    (1124, 1188,),
-    (1164, 1156, 1180,),
+    (1123, 124,),
+    (1163, 188, 164, 1108,),
+    (1155, 1171, 172, 156, 1180, 1116,),
+    (1124,),
+    (1188, 1164, 1172, 1156,),
 )
 
 PIECES = (
     ("share", 1),
     ("pool", 4),
     ("group", 2),
+    ("project half", 8),
     ("project", 8),
     ("norm", 4),
     ("last", 1),
@@ -128,6 +139,8 @@
 TOTAL = sum(count for _, count in PIECES)
 
 AXIS = {"x": "fs_2", "y": "fs_1"}
+GELU_A = 0.7978845608028654
+GELU_B = 0.044715
 
 X_GAIN, X_SCALE, X_INPUT, X_MIXER, X_FINAL = 0, 1, 2, 3, 4
 
@@ -376,11 +389,22 @@
         out = dot_nt(mixed[:, columns], right) * pool_scale[pl.ds(g, 1), :]
         normed[:, columns] = out.astype(BF16)
 
-    def project(side, block):
-        right = jnp.concatenate(
-            [w[U_OUT + k, side, block].reshape(256, PAIR) for k in range(4)], axis=1
-        )
-        part[side, :, block_of(block)] = dot_nt(normed[:, 0:HALF], right).astype(BF16)
+    def project(side, block, units, columns):
+        right = jnp.concatenate([w[u, side, block].reshape(256, PAIR) for u in units], axis=1)
+        return dot_nt(normed[:, columns], right)
+
+    def sides(k):
+        return jnp.where(k < 4, mate, tp), lax.rem(k, 4)
+
+    def project_half(k):
+        side, block = sides(k)
+        acc[:, block_of(k)] = project(side, block, range(U_OUT, U_OUT + 2), slice(0, 512))
+
+    def project_rest(k):
+        side, block = sides(k)
+        rest = project(side, block, range(U_OUT + 2, U_OUT + 4), slice(512, HALF))
+        part[side, :, block_of(block)] = (acc[:, block_of(k)] + rest).astype(BF16)
+        mixer_piece(side, block).start()
 
     def mixer_piece(side, block):
         columns = block_of(block)
@@ -415,10 +439,13 @@
         at = lax.broadcasted_iota(jnp.int32, lifted.shape, 0)
         before = jnp.where(at == 0, 0.0, pltpu.roll(lifted, 1, 0))
         after = jnp.where(at == LENGTH - 1, 0.0, pltpu.roll(lifted, LENGTH - 1, 0))
-        return jax.nn.gelu(taps[0:1] * before + taps[1:2] * lifted + taps[2:3] * after)
+        conv = taps[0:1] * before + taps[1:2] * lifted + taps[2:3] * after
+        inner = conv * (GELU_A + (GELU_A * GELU_B) * (conv * conv))
+        return conv + conv * jnp.tanh(inner)
 
     def hidden_of(active, gate_raw, columns):
-        return (active * (gate_raw * gate_scale[columns].reshape(1, -1))).astype(BF16)
+        half_scale = 0.5 * gate_scale[columns].reshape(1, -1)
+        return (active * (gate_raw * half_scale)).astype(BF16)
 
     def slab(u):
         return w[u].reshape(WIDTH, PAIR)
@@ -485,12 +512,6 @@
 
             pool(s)
 
-        def projecting(k):
-            side = jnp.where(k < 4, mate, tp)
-            block = lax.rem(k, 4)
-            project(side, block)
-            mixer_piece(side, block).start()
-
         def norming(s):
             @pl.when(s == 0)
             def _():
@@ -510,7 +531,8 @@
         during("share", share)
         during("pool", pooling)
         during("group", group)
-        during("project", projecting)
+        during("project half", project_half)
+        during("project", project_rest)
         during("norm", norming)
         during("last", feed_last)
         again = starts["feed again"][0]

time: 99.7 us -> 99.5 us (level)
  no operation moved by 1% of the time
where the time goes in v7:
time: 99.5 us; the launch traced here: 99.4 us
  Pallas kernels  98.1 us (99%)
  local copies, waits for them, and re-layouts  1.32 us (1%)
    pallas_call x1, Pallas kernels, layer(): pl.pallas_call(kernel, out_shape=pltpu.VMEM((ROWS, HALF), BF16), in_specs...  98.1 us

profile of v7, /device:TPU:1, one launch (start us, length us, event | category | flops | bytes accessed | tf_op | source)
XLA Modules:
  0.0 99.4 jit_solution(16595136984143322030)
XLA Ops:
  0.0 98.1 %shard_map.136 = bf16[1024,1024]{1,0:T(8,128)(2,1)S(1)} custom-call(bf16[1024,1024]{1,0:T(8,128)(2,1)} %x_hbm.1, f32[2,16,512]{2,1,0:T(8,128)} %bitcast.5, f32[64,1024]{1,0:T(8,128)} %bitcast.4, f32[64,1408]{1,0:T(8,128)} %up_hbm.1, f32[64,1408]{1,0:T(8,128)} %gate_hbm.1, f32[64,1408]{1,0:T(8,128)} %bitcast.3, bf16[1024]{0:T(1024)(128)(2,1)} %mix_gain_hbm.1, ...), custom_call_target="tpu_custom_call" | custom-call | tf_op jit(solution)/shard_map/pallas_call | solution.py:612
  98.1 1.3 %copy.16 = bf16[1024,1024]{1,0:T(8,128)(2,1)} copy(bf16[1024,1024]{1,0:T(8,128)(2,1)S(1)} %shard_map.136) | data formatting | bytes 4194304

commit v8 on v7

--- a/solution.py
+++ b/solution.py
@@ -497,8 +497,6 @@
                 body(m - first_one)
 
         def share(_):
-            for load in loads[5:]:
-                load.wait()
             across(x_hbm, x.at[tp], X_INPUT).start()
             across(gain_hbm, mate_gain, X_GAIN).start()
             across(out_scale_hbm, mate_out_scale, X_SCALE).start()
@@ -506,6 +504,8 @@
         def pooling(s):
             @pl.when(s == 0)
             def _():
+                for load in loads[5:]:
+                    load.wait()
                 across(x_hbm, x.at[mate], X_INPUT).wait_recv()
                 across(gain_hbm, mate_gain, X_GAIN).wait_recv()
                 across(out_scale_hbm, mate_out_scale, X_SCALE).wait_recv()

time: 99.5 us -> 99.4 us (level)
  no operation moved by 1% of the time
where the time goes in v8:
time: 99.4 us; the launch traced here: 99.2 us
  Pallas kernels  97.9 us (98%)
  local copies, waits for them, and re-layouts  1.32 us (1%)
    pallas_call x1, Pallas kernels, layer(): pl.pallas_call(kernel, out_shape=pltpu.VMEM((ROWS, HALF), BF16), in_specs...  97.9 us

profile of v8, /device:TPU:1, one launch (start us, length us, event | category | flops | bytes accessed | tf_op | source)
XLA Modules:
  0.0 99.2 jit_solution(11348677969721028088)
XLA Ops:
  0.0 97.9 %shard_map.136 = bf16[1024,1024]{1,0:T(8,128)(2,1)S(1)} custom-call(bf16[1024,1024]{1,0:T(8,128)(2,1)} %x_hbm.1, f32[2,16,512]{2,1,0:T(8,128)} %bitcast.5, f32[64,1024]{1,0:T(8,128)} %bitcast.4, f32[64,1408]{1,0:T(8,128)} %up_hbm.1, f32[64,1408]{1,0:T(8,128)} %gate_hbm.1, f32[64,1408]{1,0:T(8,128)} %bitcast.3, bf16[1024]{0:T(1024)(128)(2,1)} %mix_gain_hbm.1, ...), custom_call_target="tpu_custom_call" | custom-call | tf_op jit(solution)/shard_map/pallas_call | solution.py:612
  97.9 1.3 %copy.16 = bf16[1024,1024]{1,0:T(8,128)(2,1)} copy(bf16[1024,1024]{1,0:T(8,128)(2,1)S(1)} %shard_map.136) | data formatting | bytes 4194304
